TPU v7x, 512 devices: a 4x2x32 block of a 4x8x32 slice. The times are simulated.
512 devices in a mesh: grp: 2 (over y), fs: 32 (over z), tp: 8 (over x, core).
Axes of the slice: x: 4, y: 2, z: 32, core: 2. Of those that a mesh axis runs over, the one named last changes fastest.
The devices are a block of a 4x8x32 slice.
Arguments:
- tokens: bfloat16 [16384, 2048], P(('grp', 'fs'), 'tp'), parts along dimension 0, may hold values from -6 to 6
- recurrent_norm_gain: float32 [2048], replicated, may hold values from 0.1 to 1.9
- feedforward_norm_gain: float32 [2048], replicated, may hold values from 0.1 to 1.9
- gate_projection_weight: bfloat16 [2048, 2048], P('fs', 'tp'), may hold values from -0.125 to 0.125
- recurrent_projection_weight: bfloat16 [2048, 2048], P('fs', 'tp'), may hold values from -0.125 to 0.125
- convolution_kernel: bfloat16 [4, 2048], P(None, 'tp'), may hold values from -3 to 3
- decay_gate_matrix: bfloat16 [16, 128, 128], P('tp'), may hold values from -0.5 to 0.5
- input_gate_matrix: bfloat16 [16, 128, 128], P('tp'), may hold values from -0.5 to 0.5
- base_decay_logit: float32 [2048], P('tp'), may hold values from 3 to 9
- extra_log_decay: float32 [16384], P(('grp', 'fs')), parts along dimension 0, may hold values from -0.7 to 0
- output_projection_weight: bfloat16 [2048, 2048], P('tp', 'fs'), may hold values from -0.125 to 0.125
- up_projection_weight: bfloat16 [2048, 8192], P('fs', 'tp'), may hold values from -0.125 to 0.125
- down_projection_weight: bfloat16 [8192, 2048], P('tp', 'fs'), may hold values from -0.0625 to 0.0625
Outputs:
- layer_out: bfloat16 [16384, 2048], P(('grp', 'fs'), 'tp'), parts along dimension 0
There are 2 independent parts, one for each index of `grp`. A program takes and returns all parts, laid end to end along the dimension named above; an argument that names none is the same for every part. Nothing has to cross between parts.
All inputs are finite; a program needn't handle non-finite values.
Results may differ from a plain program's by a relative error of at most 0.018.
Values may be sent and summed in bfloat16 or wider, within the bound.
No kernel may reach another device: no remote copies, remote signals or barrier semaphores. Data moves between devices by JAX's collectives and lax.ppermute only.
A program may use at most 64 MiB of HBM per device.

v0:
```python
import jax
import jax.numpy as jnp
from jax import lax
from jax.experimental import pallas as pl
from jax.experimental.pallas import tpu as pltpu
from jax.sharding import PartitionSpec as P


RUN = 4
CHUNK = 256
PIECES = 2


def from_everyone(x, axis):
    copies = jnp.broadcast_to(x, (lax.axis_size(axis), *x.shape))
    return lax.all_to_all(copies, axis, split_axis=0, concat_axis=0, tiled=True)


def parts_of_all_groups(mine):
    groups = lax.axis_size("grp")
    up = [(k, (k + 1) % groups) for k in range(groups)]
    down = [(k, (k - 1) % groups) for k in range(groups)]
    behind = [mine]
    ahead = []
    for _ in range(groups // 2):
        behind.append(lax.ppermute(behind[-1], "grp", up))
    for _ in range((groups - 1) // 2):
        ahead.append(lax.ppermute(ahead[-1] if ahead else mine, "grp", down))
    return behind + ahead[::-1]


def gather_early(shard, waiting):
    rows, cols = shard.shape
    groups = lax.axis_size("grp")
    me = lax.axis_index("grp")
    ring = lax.axis_size("fs")
    runs = ring // RUN
    part = lax.dynamic_slice_in_dim(shard, me * (rows // groups), rows // groups, 0)
    strided = [[k + RUN * j for j in range(runs)] for k in range(RUN)]
    close = [[RUN * m + k for k in range(RUN)] for m in range(runs)]
    level = lax.all_gather(part, "fs", axis=0, tiled=True, axis_index_groups=strided)
    pieces = PIECES
    wide = cols // pieces
    done = []
    for k in range(pieces):
        piece = level[:, k * wide : (k + 1) * wide]
        got = lax.all_to_all(
            jnp.broadcast_to(piece, (RUN, *piece.shape)),
            "fs",
            0,
            0,
            tiled=True,
            axis_index_groups=close,
        ).reshape(-1, wide)
        if k == pieces - 1:
            got, waiting = lax.optimization_barrier((got, waiting))
        done.append(parts_of_all_groups(got))
    return done, waiting


def shifted(x, by, fill):
    rows = lax.broadcasted_iota(jnp.int32, x.shape, 0)
    return jnp.where(rows >= by, pltpu.roll(x, by, 0), fill)


def recurrent_body(groups, pieces, runs, me_ref, *refs):
    parts = refs[: pieces * groups]
    (tiles, gain, taps, maps, rate, extra, out, normed, weights) = refs[
        pieces * groups :
    ]
    blocks, length, block = tiles.shape
    width = taps.shape[1]
    each = parts[0].shape[0] // (RUN * runs)
    wide = parts[0].shape[1]
    for behind in range(groups):
        place = lax.rem(me_ref[0] + groups - behind, groups) * each
        for near in range(RUN):
            for far in range(runs):
                to = pl.multiple_of((far * RUN + near) * groups * each + place, each)
                start = (near * runs + far) * each
                for piece in range(pieces):
                    weights[pl.ds(to, each), piece * wide : (piece + 1) * wide] = parts[
                        piece * groups + behind
                    ][start : start + each, :]
    squares = jnp.zeros((length, 1), jnp.float32)
    for k in range(blocks):
        v = tiles[k].astype(jnp.float32)
        squares = squares + jnp.sum(v * v, axis=-1, keepdims=True)
    inverse = lax.rsqrt(squares / (blocks * block) + 1e-06)
    for k in range(blocks):
        here = slice(k * block, (k + 1) * block)
        normed[:, here] = (tiles[k].astype(jnp.float32) * inverse * gain[:, here]).astype(
            jnp.bfloat16
        )
    recur = jnp.dot(normed[...], weights[:, :width], preferred_element_type=jnp.float32)
    gate_pre = jnp.dot(
        normed[...], weights[:, width : 2 * width], preferred_element_type=jnp.float32
    )
    gate = jax.nn.gelu(gate_pre).astype(jnp.bfloat16).astype(jnp.float32)
    recur = recur.astype(jnp.bfloat16).astype(jnp.float32)
    count = taps.shape[0]
    conv_sum = recur * taps[count - 1 : count, :].astype(jnp.float32)
    for k in range(1, count):
        conv_sum = conv_sum + shifted(recur, k, 0.0) * taps[count - 1 - k : count - k, :].astype(
            jnp.float32
        )
    conv_rows = conv_sum.astype(jnp.bfloat16)
    count = maps.shape[0] // 2
    size = width // count
    recur_gate = []
    input_rate = []
    for k in range(count):
        x = conv_rows[:, k * size : (k + 1) * size]
        recur_gate.append(jnp.dot(x, maps[k], preferred_element_type=jnp.float32))
        input_rate.append(jnp.dot(x, maps[count + k], preferred_element_type=jnp.float32))
    recur_gate = jax.nn.sigmoid(jnp.concatenate(recur_gate, axis=1))
    input_rate = jax.nn.sigmoid(jnp.concatenate(input_rate, axis=1))
    log_decay = rate[...] * recur_gate + extra[...]
    decay = jnp.exp(log_decay)
    u = -log_decay
    small = 2.0 * u * (1.0 - u * (1.0 - u * (2.0 / 3.0 - u * (1.0 / 3.0 - u * (2.0 / 15.0)))))
    lost = jnp.where(u < 0.015625, small, 1.0 - decay * decay)
    hidden = jnp.sqrt(lost) * input_rate * conv_rows.astype(jnp.float32)
    by = 1
    while by < length:
        hidden = hidden + decay * shifted(hidden, by, 0.0)
        if 2 * by < length:
            decay = decay * shifted(decay, by, 1.0)
        by *= 2
    mixed = (hidden * gate).astype(jnp.bfloat16)
    for k in range(blocks):
        out[k] = lax.dot_general(
            mixed,
            weights[k * block : (k + 1) * block, 2 * width : 3 * width],
            (((1,), (1,)), ((), ())),
            preferred_element_type=jnp.float32,
        ).astype(jnp.bfloat16)


def recurrent_block(tiles, parts, gain, taps, decay_gate, input_gate, base, extra):
    groups = len(parts[0])
    pieces = len(parts)
    runs = lax.axis_size("fs") // RUN
    me = lax.axis_index("grp")
    rate = (-8.0 * jax.nn.softplus(-base))[None, :]
    flat = [p for piece in parts for p in piece]
    blocks, length, block = tiles.shape
    vmem = pl.BlockSpec(memory_space=pltpu.VMEM)
    features = blocks * block
    cols = pieces * parts[0][0].shape[1]
    return pl.pallas_call(
        lambda *refs: recurrent_body(groups, pieces, runs, *refs),
        out_shape=jax.ShapeDtypeStruct(tiles.shape, jnp.bfloat16),
        in_specs=[pl.BlockSpec(memory_space=pltpu.SMEM)] + [vmem] * (len(flat) + 6),
        out_specs=vmem,
        scratch_shapes=[
            pltpu.VMEM((length, features), jnp.bfloat16),
            pltpu.VMEM((features, cols), jnp.bfloat16),
        ],
        cost_estimate=pl.CostEstimate(
            flops=2 * length * features * cols,
            transcendentals=6 * length * taps.shape[1],
            bytes_accessed=2 * (features * cols + 2 * length * features),
        ),
        compiler_params=pltpu.CompilerParams(vmem_limit_bytes=40 << 20),
        name="recurrent",
    )(
        jnp.full((1,), me, jnp.int32),
        *flat,
        tiles,
        gain[None, :],
        taps,
        jnp.concatenate([decay_gate, input_gate]),
        rate,
        extra[:, None],
    )


def feed_forward_body(tiles, gain, weights, out, normed, total, held, arrived):
    blocks, length, block = tiles.shape
    steps = held.shape[0] // 2
    copies = [
        pltpu.make_async_copy(
            weights.at[:, k * CHUNK : (k + 1) * CHUNK], held.at[k], arrived.at[k]
        )
        for k in range(2 * steps)
    ]
    for k in range(steps):
        copies[k].start()
        copies[steps + k].start()
    squares = jnp.zeros((length, 1), jnp.float32)
    for k in range(blocks):
        v = tiles[k].astype(jnp.float32)
        squares = squares + jnp.sum(v * v, axis=-1, keepdims=True)
    inverse = lax.rsqrt(squares / (blocks * block) + 1e-06)
    for k in range(blocks):
        here = slice(k * block, (k + 1) * block)
        normed[:, here] = (tiles[k].astype(jnp.float32) * inverse * gain[:, here]).astype(
            jnp.bfloat16
        )
    for step in range(steps):
        copies[step].wait()
        upward = jnp.dot(normed[...], held[step], preferred_element_type=jnp.float32)
        positive = jnp.maximum(upward, 0.0)
        squared = (positive * positive).astype(jnp.bfloat16)
        copies[steps + step].wait()
        for k in range(blocks):
            product = lax.dot_general(
                squared,
                held[steps + step, k * block : (k + 1) * block, :],
                (((1,), (1,)), ((), ())),
                preferred_element_type=jnp.float32,
            )
            product = product if step == 0 else total[k] + product
            if step < steps - 1:
                total[k] = product
            else:
                out[k] = product.astype(jnp.bfloat16)


def feed_forward(tiles, gain, weights):
    _, length, _ = tiles.shape
    features, both = weights.shape
    vmem = pl.BlockSpec(memory_space=pltpu.VMEM)
    return pl.pallas_call(
        feed_forward_body,
        out_shape=jax.ShapeDtypeStruct(tiles.shape, jnp.bfloat16),
        in_specs=[vmem, vmem, pl.BlockSpec(memory_space=pltpu.HBM)],
        out_specs=vmem,
        scratch_shapes=[
            pltpu.VMEM((length, features), jnp.bfloat16),
            pltpu.VMEM(tiles.shape, jnp.float32),
            pltpu.VMEM((both // CHUNK, features, CHUNK), jnp.bfloat16),
            pltpu.SemaphoreType.DMA((both // CHUNK,)),
        ],
        cost_estimate=pl.CostEstimate(
            flops=2 * length * features * both,
            transcendentals=length,
            bytes_accessed=2 * (features * both + 2 * length * features),
        ),
        compiler_params=pltpu.CompilerParams(vmem_limit_bytes=40 << 20),
        name="feed_forward",
    )(tiles, gain[None, :], pltpu.with_memory_space_constraint(weights, pltpu.HBM))


def per_device(
    tokens,
    recurrent_norm_gain,
    feedforward_norm_gain,
    gate_projection_weight,
    recurrent_projection_weight,
    convolution_kernel,
    decay_gate_matrix,
    input_gate_matrix,
    base_decay_logit,
    extra_log_decay,
    output_projection_weight,
    up_projection_weight,
    down_projection_weight,
):
    late = jnp.concatenate([up_projection_weight, down_projection_weight.T], axis=1)
    late, tokens = lax.optimization_barrier((late, tokens))
    late_whole = lax.all_gather(late, "fs", axis=0, tiled=True)
    early = jnp.concatenate(
        [recurrent_projection_weight, gate_projection_weight, output_projection_weight.T], axis=1
    )
    parts, held = gather_early(early, tokens)
    token_tiles = from_everyone(held, "tp")
    partials = recurrent_block(
        token_tiles,
        parts,
        recurrent_norm_gain,
        convolution_kernel,
        decay_gate_matrix,
        input_gate_matrix,
        base_decay_logit,
        extra_log_decay,
    )
    arrived = lax.all_to_all(partials, "tp", 0, 0, tiled=True)
    residual = (
        tokens.astype(jnp.float32) + jnp.sum(arrived.astype(jnp.float32), axis=0)
    ).astype(jnp.bfloat16)
    down_terms = feed_forward(from_everyone(residual, "tp"), feedforward_norm_gain, late_whole)
    returned = lax.all_to_all(down_terms, "tp", 0, 0, tiled=True)
    return (
        residual.astype(jnp.float32) + jnp.sum(returned.astype(jnp.float32), axis=0)
    ).astype(jnp.bfloat16)


def solution(mesh):
    placed = (
        P(("grp", "fs"), "tp"),
        P(),
        P(),
        P("fs", "tp"),
        P("fs", "tp"),
        P(None, "tp"),
        P("tp", None, None),
        P("tp", None, None),
        P("tp"),
        P(("grp", "fs")),
        P("tp", "fs"),
        P("fs", "tp"),
        P("tp", "fs"),
    )

    return jax.shard_map(
        per_device, mesh=mesh, in_specs=placed, out_specs=P(("grp", "fs"), "tp"), check_vma=False
    )
```

profile of v0, /device:TPU:33, one launch (start us, length us, event | category | flops | bytes accessed | tf_op | source)
XLA Modules:
  0.0 273.6 jit_solution(17290786761819996936)
XLA Ops:
  6.6 1.7 pad_maximum_fusion
  8.2 0.1 all-gather.2.cloned.1.call-update
  8.3 0.8 fusion.1
  9.1 74.8 %all_gather.6 = bf16[256,768]{1,0:T(8,128)(2,1)S(1)} all-gather(bf16[32,768]{1,0:T(8,128)(2,1)S(1)} %fusion.1), channel_id=1, replica_groups={{0,32,64,96,128,160,192,224},{8,40,72,104,136,168,200,232},{16,48,80,11..., dimensions={0}, use_global_device_ids=true | all-gather | bytes 442368 | tf_op jit(solution)/shard_map/all_gather | solution.py:41
  83.9 0.1 broadcast_in_dim.29
  84.0 0.0 copy-start.4
  84.0 29.4 %all_to_all.30 = bf16[4,256,384]{2,1,0:T(8,128)(2,1)S(1)} all-to-all(bf16[4,256,384]{2,1,0:T(8,128)(2,1)S(1)} %broadcast_in_dim.29), channel_id=1, replica_groups={{0,8,16,24},{32,40,48,56},{64,72,80,88},{96,104,112,120},{128,136,144,1..., dimensions={0} | all-to-all | bytes 1572864 | tf_op jit(solution)/shard_map/all_to_all | solution.py:47
  113.3 1.0 broadcast_in_dim.28
  114.4 4.2 %all-to-all-start = ((bf16[4,256,384]{2,1,0:T(8,128)(2,1)}), bf16[4,256,384]{2,1,0:T(8,128)(2,1)S(1)}, u32[]{:S(2)}, u32[]{:S(2)}) async-start(bf16[4,256,384]{2,1,0:T(8,128)(2,1)} %broadcast_in_dim.28), calls=%async_computation | async-start | bytes 1572864 | tf_op jit(solution)/shard_map/all_to_all | solution.py:47
  118.6 27.1 %all-to-all-done = bf16[4,256,384]{2,1,0:T(8,128)(2,1)S(1)} async-done(((bf16[4,256,384]{2,1,0:T(8,128)(2,1)}), bf16[4,256,384]{2,1,0:T(8,128)(2,1)S(1)}, u32[]{:S(2)}, u32[]{:S(2)}) %all-to-all-start) | async-done | bytes 786464 | tf_op jit(solution)/shard_map/all_to_all | solution.py:47
  145.7 1.1 broadcast_in_dim.30
  146.9 12.1 %all-to-all-start.2 = ((bf16[8,256,256]{2,1,0:T(8,128)(2,1)}), bf16[8,256,256]{2,1,0:T(8,128)(2,1)S(1)}, u32[]{:S(2)}, u32[]{:S(2)}) async-start(bf16[8,256,256]{2,1,0:T(8,128)(2,1)} %broadcast_in_dim.30), calls=%async_computation.2 | async-start | bytes 2097152 | tf_op jit(solution)/shard_map/all_to_all | solution.py:16
  159.0 3.6 %collective-permute-start.1 = (bf16[1024,384]{1,0:T(8,128)(2,1)S(1)}, bf16[1024,384]{1,0:T(8,128)(2,1)S(1)}, u32[]{:S(2)}, u32[]{:S(2)}) collective-permute-start(bf16[1024,384]{1,0:T(8,128)(2,1)S(1)} %bitcast.9), channel_id=1, source_target_pairs={{0,256},{256,0},{1,257},{257,1},{2,258},{258,2},{3,259},{259,3},{4... | collective-permute-start | bytes 2359304 | tf_op jit(solution)/shard_map/ppermute | solution.py:26
  162.6 2.0 collective-permute-start
  164.6 0.1 copy.14.refs_10_
  164.7 1.5 pad_maximum_fusion.1.refs_8_
  166.2 0.7 fusion.2
  166.9 13.6 %collective-permute-done.1.refs_4_ = bf16[1024,384]{1,0:T(8,128)(2,1)S(1)} collective-permute-done((bf16[1024,384]{1,0:T(8,128)(2,1)S(1)}, bf16[1024,384]{1,0:T(8,128)(2,1)S(1)}, u32[]{:S(2)}, u32[]{:S(2)}) %collective-permute-start.1) | collective-permute-done | bytes 786464 | tf_op jit(solution)/shard_map/ppermute | solution.py:26
  180.5 16.9 %collective-permute-done.refs_2_ = bf16[1024,384]{1,0:T(8,128)(2,1)} collective-permute-done((bf16[1024,384]{1,0:T(8,128)(2,1)S(1)}, bf16[1024,384]{1,0:T(8,128)(2,1)}, u32[]{:S(2)}, u32[]{:S(2)}) %collective-permute-start) | collective-permute-done | bytes 786464 | tf_op jit(solution)/shard_map/ppermute | solution.py:26
  197.4 0.0 copy-start
  197.4 0.9 copy-done
  198.3 3.5 %recurrent.1 = bf16[8,256,256]{2,1,0:T(8,128)(2,1)S(1)} custom-call(s32[1]{0:T(128)} %bitcast.1.refs_0_, bf16[1024,384]{1,0:T(8,128)(2,1)S(1)} %bitcast.12, bf16[1024,384]{1,0:T(8,128)(2,1)} %collective-permute-done.refs_2_, bf16[1024,384]{1,0:T(8,128)(2,1)S(1)} %bitcast.10, bf16[1024,384]{1,0:T(8,128)(2,1)S(1)} %collective-permute-done.1.refs_4_, ...), custom_call_target="tpu_custom_call" | custom-call | flops 805306368 | bytes 5242880 | tf_op jit(solution)/shard_map/recurrent/pallas_call | solution.py:151
  201.8 0.0 copy-start.5
  201.8 20.0 %all_to_all.31 = bf16[8,256,256]{2,1,0:T(8,128)(2,1)S(1)} all-to-all(bf16[8,256,256]{2,1,0:T(8,128)(2,1)S(1)} %recurrent.1), channel_id=1, replica_groups=mesh['grp'=2,'fs'=32,'tp'=8] {'tp'}, dimensions={0} | all-to-all | bytes 2097152 | tf_op jit(solution)/shard_map/all_to_all | solution.py:279
  221.8 0.1 convert_reduce_fusion.1
  222.0 0.0 copy-start.2
  222.0 0.1 broadcast_in_dim.34
  222.1 18.5 %all_to_all.32.tiles = bf16[8,256,256]{2,1,0:T(8,128)(2,1)S(1)} all-to-all(bf16[8,256,256]{2,1,0:T(8,128)(2,1)S(1)} %broadcast_in_dim.34), channel_id=1, replica_groups=mesh['grp'=2,'fs'=32,'tp'=8] {'tp'}, dimensions={0} | all-to-all | bytes 2097152 | tf_op jit(solution)/shard_map/all_to_all | solution.py:16
  240.6 6.8 %feed_forward.1 = bf16[8,256,256]{2,1,0:T(8,128)(2,1)S(1)} custom-call(bf16[8,256,256]{2,1,0:T(8,128)(2,1)S(1)} %all_to_all.32.tiles, f32[1,2048]{1,0:T(1,128)S(1)} %bitcast.14, bf16[2048,2048]{1,0:T(8,128)(2,1)} %all-gather.2.cloned.1.call-done.weights), custom_call_target="tpu_custom_call" | custom-call | flops 2147483648 | bytes 10485760 | tf_op jit(solution)/shard_map/feed_forward/pallas_call | solution.py:225
  247.4 18.5 %all_to_all.33 = bf16[8,256,256]{2,1,0:T(8,128)(2,1)S(1)} all-to-all(bf16[8,256,256]{2,1,0:T(8,128)(2,1)S(1)} %feed_forward.1), channel_id=1, replica_groups=mesh['grp'=2,'fs'=32,'tp'=8] {'tp'}, dimensions={0} | all-to-all | bytes 2097152 | tf_op jit(solution)/shard_map/all_to_all | solution.py:284
  265.9 0.1 convert_reduce_fusion
  266.0 0.7 add_convert_fusion
  (14 shorter events, 0.1 us)
Async XLA Ops:
  6.5 234.0 %all-gather.2.cloned.1.call-start = ((), (), s32[]{:S(2)}) async-start(), calls=%async_computation.6 | async-start | bytes 8650752 | tf_op jit(solution)/shard_map/all_gather | solution.py:263
  84.0 61.8 %copy-start.4 = (bf16[256,256]{1,0:T(8,128)(2,1)S(1)}, bf16[256,256]{1,0:T(8,128)(2,1)}, u32[]{:S(2)}) copy-start(bf16[256,256]{1,0:T(8,128)(2,1)} %param.13) | copy-start | bytes 393220
  114.4 50.2 %copy-start.6 = (f32[256]{0:T(256)S(1)}, f32[256]{0:T(256)}, u32[]{:S(2)}) copy-start(f32[256]{0:T(256)} %param.22) | copy-start | bytes 3076
  114.4 31.4 %all-to-all-start = ((bf16[4,256,384]{2,1,0:T(8,128)(2,1)}), bf16[4,256,384]{2,1,0:T(8,128)(2,1)S(1)}, u32[]{:S(2)}, u32[]{:S(2)}) async-start(bf16[4,256,384]{2,1,0:T(8,128)(2,1)} %broadcast_in_dim.28), calls=%async_computation | async-start | bytes 1572864 | tf_op jit(solution)/shard_map/all_to_all | solution.py:47
  118.6 78.8 %copy-start.1 = (f32[2048]{0:T(1024)S(1)}, f32[2048]{0:T(1024)}, u32[]{:S(2)}) copy-start(f32[2048]{0:T(1024)} %param.14) | copy-start | bytes 24580
  118.6 78.8 %copy-start.3 = (bf16[4,256]{1,0:T(4,128)(2,1)S(1)}, bf16[4,256]{1,0:T(4,128)(2,1)}, u32[]{:S(2)}) copy-start(bf16[4,256]{1,0:T(4,128)(2,1)} %refs_7_.1) | copy-start | bytes 6148
  146.9 50.5 %all-to-all-start.2 = ((bf16[8,256,256]{2,1,0:T(8,128)(2,1)}), bf16[8,256,256]{2,1,0:T(8,128)(2,1)S(1)}, u32[]{:S(2)}, u32[]{:S(2)}) async-start(bf16[8,256,256]{2,1,0:T(8,128)(2,1)} %broadcast_in_dim.30), calls=%async_computation.2 | async-start | bytes 2097152 | tf_op jit(solution)/shard_map/all_to_all | solution.py:16
  159.0 21.5 %collective-permute-start.1 = (bf16[1024,384]{1,0:T(8,128)(2,1)S(1)}, bf16[1024,384]{1,0:T(8,128)(2,1)S(1)}, u32[]{:S(2)}, u32[]{:S(2)}) collective-permute-start(bf16[1024,384]{1,0:T(8,128)(2,1)S(1)} %bitcast.9), channel_id=1, source_target_pairs={{0,256},{256,0},{1,257},{257,1},{2,258},{258,2},{3,259},{259,3},{4... | collective-permute-start | bytes 2359304 | tf_op jit(solution)/shard_map/ppermute | solution.py:26
  162.6 34.8 %collective-permute-start = (bf16[1024,384]{1,0:T(8,128)(2,1)S(1)}, bf16[1024,384]{1,0:T(8,128)(2,1)}, u32[]{:S(2)}, u32[]{:S(2)}) collective-permute-start(bf16[1024,384]{1,0:T(8,128)(2,1)S(1)} %bitcast.11), channel_id=1, source_target_pairs={{0,256},{256,0},{1,257},{257,1},{2,258},{258,2},{3,259},{259,3},{4... | collective-permute-start | bytes 2359304 | tf_op jit(solution)/shard_map/ppermute | solution.py:26
  197.4 0.9 copy-start
  201.8 20.1 %copy-start.5 = (bf16[256,256]{1,0:T(8,128)(2,1)S(1)}, bf16[256,256]{1,0:T(8,128)(2,1)}, u32[]{:S(2)}) copy-start(bf16[256,256]{1,0:T(8,128)(2,1)} %param.13) | copy-start | bytes 393220
  222.0 18.6 %copy-start.2 = (f32[2048]{0:T(1024)S(1)}, f32[2048]{0:T(1024)}, u32[]{:S(2)}) copy-start(f32[2048]{0:T(1024)} %param.15) | copy-start | bytes 24580
Sparse Core Ops, SparseCore 0:
  9.4 193.9 all-gather.1
where the time goes:
time: 274 us
  blocking collectives  161 us (59%)
  waiting for transfers between devices  57.6 us (21%)
  starting transfers between devices  21.9 us (8%)
  between operations  13.5 us (5%)
  Pallas kernels  10.4 us (4%)
  other arithmetic  5.68 us (2%)
  local copies, waits for them, and re-layouts  3.39 us (1%)
    all_gather x1, blocking collectives, gather_early(): lax.all_gather(part, 'fs', axis=0, tiled=True, axis_index_groups=strided)  74.8 us
    ppermute x2, waiting for transfers between devices, parts_of_all_groups(): behind.append(lax.ppermute(behind[-1], 'grp', up))  30.4 us
    all_to_all x1, blocking collectives, gather_early(): lax.all_to_all(jnp.broadcast_to(piece, (RUN, *piece.shape)), 'fs', 0, 0,...  29.4 us
    all_to_all x1, waiting for transfers between devices, gather_early(): lax.all_to_all(jnp.broadcast_to(piece, (RUN, *piece.shape)), 'fs', 0, 0,...  27.1 us
    all_to_all x1, blocking collectives, per_device(): arrived = lax.all_to_all(partials, 'tp', 0, 0, tiled=True)  20 us
    all_to_all x1, blocking collectives, from_everyone(): return lax.all_to_all(copies, axis, split_axis=0, concat_axis=0, tiled=True)  18.5 us
    all_to_all x1, blocking collectives, per_device(): returned = lax.all_to_all(down_terms, 'tp', 0, 0, tiled=True)  18.5 us
    all_to_all x1, starting transfers between devices, from_everyone(): return lax.all_to_all(copies, axis, split_axis=0, concat_axis=0, tiled=True)  12.1 us
  transfers between devices with their start and end apart: 5, of which 3 were waited for; matrix products, arithmetic and copies ran while one was open for 2% of the time, Pallas kernels for 1%

commit v1 on v0

--- a/solution.py
+++ b/solution.py
@@ -7,13 +7,63 @@
 
 
 RUN = 4
+CORES = 2
 CHUNK = 256
 PIECES = 2
 
 
-def from_everyone(x, axis):
-    copies = jnp.broadcast_to(x, (lax.axis_size(axis), *x.shape))
-    return lax.all_to_all(copies, axis, split_axis=0, concat_axis=0, tiled=True)
+def same_core():
+    members = lax.axis_size("tp")
+    return [list(range(c, members, CORES)) for c in range(CORES)]
+
+
+def with_partner(x):
+    members = lax.axis_size("tp")
+    return lax.ppermute(x, "tp", [(k, k + 1 - 2 * (k % CORES)) for k in range(members)])
+
+
+def from_everyone(x):
+    groups = same_core()
+    copies = jnp.broadcast_to(x, (len(groups[0]), *x.shape))
+    mine = lax.all_to_all(copies, "tp", 0, 0, tiled=True, axis_index_groups=groups)
+    return mine, with_partner(mine)
+
+
+def summed_over_peers(keep, give):
+    pair = keep.astype(jnp.float32) + with_partner(give).astype(jnp.float32)
+    tiles = lax.all_to_all(
+        pair.astype(jnp.bfloat16), "tp", 0, 0, tiled=True, axis_index_groups=same_core()
+    )
+    return jnp.sum(tiles.astype(jnp.float32), axis=0)
+
+
+def norm_rows(core, mine, other, gain, normed):
+    half, length, block = mine.shape
+    blocks = CORES * half
+
+    def tile(k):
+        first = mine[k // CORES].astype(jnp.float32)
+        second = other[k // CORES].astype(jnp.float32)
+        return jnp.where(core == k % CORES, first, second)
+
+    squares = jnp.zeros((length, 1), jnp.float32)
+    for k in range(blocks):
+        v = tile(k)
+        squares = squares + jnp.sum(v * v, axis=-1, keepdims=True)
+    inverse = lax.rsqrt(squares / (blocks * block) + 1e-06)
+    for k in range(blocks):
+        here = slice(k * block, (k + 1) * block)
+        normed[:, here] = (tile(k) * inverse * gain[:, here]).astype(jnp.bfloat16)
+
+
+def put(core, k, value, keep, give):
+    @pl.when(core == k % CORES)
+    def _():
+        keep[k // CORES] = value
+
+    @pl.when(core != k % CORES)
+    def _():
+        give[k // CORES] = value
 
 
 def parts_of_all_groups(mine):
@@ -44,14 +94,7 @@
     done = []
     for k in range(pieces):
         piece = level[:, k * wide : (k + 1) * wide]
-        got = lax.all_to_all(
-            jnp.broadcast_to(piece, (RUN, *piece.shape)),
-            "fs",
-            0,
-            0,
-            tiled=True,
-            axis_index_groups=close,
-        ).reshape(-1, wide)
+        got = lax.all_gather(piece, "fs", axis=0, tiled=True, axis_index_groups=close)
         if k == pieces - 1:
             got, waiting = lax.optimization_barrier((got, waiting))
         done.append(parts_of_all_groups(got))
@@ -65,10 +108,12 @@
 
 def recurrent_body(groups, pieces, runs, me_ref, *refs):
     parts = refs[: pieces * groups]
-    (tiles, gain, taps, maps, rate, extra, out, normed, weights) = refs[
+    (mine, other, gain, taps, maps, rate, extra, keep, give, normed, weights) = refs[
         pieces * groups :
     ]
-    blocks, length, block = tiles.shape
+    half, length, block = mine.shape
+    blocks = CORES * half
+    core = me_ref[1]
     width = taps.shape[1]
     each = parts[0].shape[0] // (RUN * runs)
     wide = parts[0].shape[1]
@@ -82,16 +127,7 @@
                     weights[pl.ds(to, each), piece * wide : (piece + 1) * wide] = parts[
                         piece * groups + behind
                     ][start : start + each, :]
-    squares = jnp.zeros((length, 1), jnp.float32)
-    for k in range(blocks):
-        v = tiles[k].astype(jnp.float32)
-        squares = squares + jnp.sum(v * v, axis=-1, keepdims=True)
-    inverse = lax.rsqrt(squares / (blocks * block) + 1e-06)
-    for k in range(blocks):
-        here = slice(k * block, (k + 1) * block)
-        normed[:, here] = (tiles[k].astype(jnp.float32) * inverse * gain[:, here]).astype(
-            jnp.bfloat16
-        )
+    norm_rows(core, mine, other, gain, normed)
     recur = jnp.dot(normed[...], weights[:, :width], preferred_element_type=jnp.float32)
     gate_pre = jnp.dot(
         normed[...], weights[:, width : 2 * width], preferred_element_type=jnp.float32
@@ -129,30 +165,31 @@
         by *= 2
     mixed = (hidden * gate).astype(jnp.bfloat16)
     for k in range(blocks):
-        out[k] = lax.dot_general(
+        product = lax.dot_general(
             mixed,
             weights[k * block : (k + 1) * block, 2 * width : 3 * width],
             (((1,), (1,)), ((), ())),
             preferred_element_type=jnp.float32,
-        ).astype(jnp.bfloat16)
+        )
+        put(core, k, product.astype(jnp.bfloat16), keep, give)
 
 
 def recurrent_block(tiles, parts, gain, taps, decay_gate, input_gate, base, extra):
     groups = len(parts[0])
     pieces = len(parts)
     runs = lax.axis_size("fs") // RUN
-    me = lax.axis_index("grp")
+    place = jnp.stack([lax.axis_index("grp"), lax.axis_index("tp") % CORES]).astype(jnp.int32)
     rate = (-8.0 * jax.nn.softplus(-base))[None, :]
     flat = [p for piece in parts for p in piece]
-    blocks, length, block = tiles.shape
+    half, length, block = tiles[0].shape
     vmem = pl.BlockSpec(memory_space=pltpu.VMEM)
-    features = blocks * block
+    features = CORES * half * block
     cols = pieces * parts[0][0].shape[1]
     return pl.pallas_call(
         lambda *refs: recurrent_body(groups, pieces, runs, *refs),
-        out_shape=jax.ShapeDtypeStruct(tiles.shape, jnp.bfloat16),
-        in_specs=[pl.BlockSpec(memory_space=pltpu.SMEM)] + [vmem] * (len(flat) + 6),
-        out_specs=vmem,
+        out_shape=[jax.ShapeDtypeStruct(tiles[0].shape, jnp.bfloat16)] * 2,
+        in_specs=[pl.BlockSpec(memory_space=pltpu.SMEM)] + [vmem] * (len(flat) + 7),
+        out_specs=[vmem] * 2,
         scratch_shapes=[
             pltpu.VMEM((length, features), jnp.bfloat16),
             pltpu.VMEM((features, cols), jnp.bfloat16),
@@ -165,9 +202,9 @@
         compiler_params=pltpu.CompilerParams(vmem_limit_bytes=40 << 20),
         name="recurrent",
     )(
-        jnp.full((1,), me, jnp.int32),
+        place,
         *flat,
-        tiles,
+        *tiles,
         gain[None, :],
         taps,
         jnp.concatenate([decay_gate, input_gate]),
@@ -176,62 +213,67 @@
     )
 
 
-def feed_forward_body(tiles, gain, weights, out, normed, total, held, arrived):
-    blocks, length, block = tiles.shape
-    steps = held.shape[0] // 2
-    copies = [
+def feed_forward_body(
+    core_ref, mine, other, gain, weights, keep, give, normed, squared, up, down, arrived
+):
+    half, _, block = mine.shape
+    blocks = CORES * half
+    core = core_ref[0]
+    hidden = squared.shape[1]
+    chunks = hidden // CHUNK
+    ups = [
+        pltpu.make_async_copy(weights.at[:, k * CHUNK : (k + 1) * CHUNK], up.at[k], arrived.at[k])
+        for k in range(chunks)
+    ]
+    downs = [
         pltpu.make_async_copy(
-            weights.at[:, k * CHUNK : (k + 1) * CHUNK], held.at[k], arrived.at[k]
+            weights.at[k * block : (k + 1) * block, hidden:], down.at[k], arrived.at[chunks + k]
         )
-        for k in range(2 * steps)
+        for k in range(blocks)
     ]
-    for k in range(steps):
-        copies[k].start()
-        copies[steps + k].start()
-    squares = jnp.zeros((length, 1), jnp.float32)
+    for copy in ups + downs:
+        copy.start()
+    norm_rows(core, mine, other, gain, normed)
+    for k in range(chunks):
+        ups[k].wait()
+        upward = jnp.dot(normed[...], up[k], preferred_element_type=jnp.float32)
+        positive = jnp.maximum(upward, 0.0)
+        squared[:, k * CHUNK : (k + 1) * CHUNK] = (positive * positive).astype(jnp.bfloat16)
     for k in range(blocks):
-        v = tiles[k].astype(jnp.float32)
-        squares = squares + jnp.sum(v * v, axis=-1, keepdims=True)
-    inverse = lax.rsqrt(squares / (blocks * block) + 1e-06)
-    for k in range(blocks):
-        here = slice(k * block, (k + 1) * block)
-        normed[:, here] = (tiles[k].astype(jnp.float32) * inverse * gain[:, here]).astype(
-            jnp.bfloat16
+        downs[k].wait()
+        product = lax.dot_general(
+            squared[...],
+            down[k],
+            (((1,), (1,)), ((), ())),
+            preferred_element_type=jnp.float32,
         )
-    for step in range(steps):
-        copies[step].wait()
-        upward = jnp.dot(normed[...], held[step], preferred_element_type=jnp.float32)
-        positive = jnp.maximum(upward, 0.0)
-        squared = (positive * positive).astype(jnp.bfloat16)
-        copies[steps + step].wait()
-        for k in range(blocks):
-            product = lax.dot_general(
-                squared,
-                held[steps + step, k * block : (k + 1) * block, :],
-                (((1,), (1,)), ((), ())),
-                preferred_element_type=jnp.float32,
-            )
-            product = product if step == 0 else total[k] + product
-            if step < steps - 1:
-                total[k] = product
-            else:
-                out[k] = product.astype(jnp.bfloat16)
+        put(core, k, product.astype(jnp.bfloat16), keep, give)
 
 
 def feed_forward(tiles, gain, weights):
-    _, length, _ = tiles.shape
+    _, length, block = tiles[0].shape
     features, both = weights.shape
+    hidden = both // 2
+    chunks = hidden // CHUNK
     vmem = pl.BlockSpec(memory_space=pltpu.VMEM)
+    core = (lax.axis_index("tp") % CORES).astype(jnp.int32).reshape(1)
     return pl.pallas_call(
         feed_forward_body,
-        out_shape=jax.ShapeDtypeStruct(tiles.shape, jnp.bfloat16),
-        in_specs=[vmem, vmem, pl.BlockSpec(memory_space=pltpu.HBM)],
-        out_specs=vmem,
+        out_shape=[jax.ShapeDtypeStruct(tiles[0].shape, jnp.bfloat16)] * 2,
+        in_specs=[
+            pl.BlockSpec(memory_space=pltpu.SMEM),
+            vmem,
+            vmem,
+            vmem,
+            pl.BlockSpec(memory_space=pltpu.HBM),
+        ],
+        out_specs=[vmem] * 2,
         scratch_shapes=[
             pltpu.VMEM((length, features), jnp.bfloat16),
-            pltpu.VMEM(tiles.shape, jnp.float32),
-            pltpu.VMEM((both // CHUNK, features, CHUNK), jnp.bfloat16),
-            pltpu.SemaphoreType.DMA((both // CHUNK,)),
+            pltpu.VMEM((length, hidden), jnp.bfloat16),
+            pltpu.VMEM((chunks, features, CHUNK), jnp.bfloat16),
+            pltpu.VMEM((features // block, block, hidden), jnp.bfloat16),
+            pltpu.SemaphoreType.DMA((chunks + features // block,)),
         ],
         cost_estimate=pl.CostEstimate(
             flops=2 * length * features * both,
@@ -240,7 +282,7 @@
         ),
         compiler_params=pltpu.CompilerParams(vmem_limit_bytes=40 << 20),
         name="feed_forward",
-    )(tiles, gain[None, :], pltpu.with_memory_space_constraint(weights, pltpu.HBM))
+    )(core, *tiles, gain[None, :], pltpu.with_memory_space_constraint(weights, pltpu.HBM))
 
 
 def per_device(
@@ -265,8 +307,8 @@
         [recurrent_projection_weight, gate_projection_weight, output_projection_weight.T], axis=1
     )
     parts, held = gather_early(early, tokens)
-    token_tiles = from_everyone(held, "tp")
-    partials = recurrent_block(
+    token_tiles = from_everyone(held)
+    keep, give = recurrent_block(
         token_tiles,
         parts,
         recurrent_norm_gain,
@@ -276,15 +318,9 @@
         base_decay_logit,
         extra_log_decay,
     )
-    arrived = lax.all_to_all(partials, "tp", 0, 0, tiled=True)
-    residual = (
-        tokens.astype(jnp.float32) + jnp.sum(arrived.astype(jnp.float32), axis=0)
-    ).astype(jnp.bfloat16)
-    down_terms = feed_forward(from_everyone(residual, "tp"), feedforward_norm_gain, late_whole)
-    returned = lax.all_to_all(down_terms, "tp", 0, 0, tiled=True)
-    return (
-        residual.astype(jnp.float32) + jnp.sum(returned.astype(jnp.float32), axis=0)
-    ).astype(jnp.bfloat16)
+    residual = (tokens.astype(jnp.float32) + summed_over_peers(keep, give)).astype(jnp.bfloat16)
+    keep, give = feed_forward(from_everyone(residual), feedforward_norm_gain, late_whole)
+    return (residual.astype(jnp.float32) + summed_over_peers(keep, give)).astype(jnp.bfloat16)
 
 
 def solution(mesh):

time: 274 us -> 244 us (0.89)
  waiting for transfers between devices: 57.6 us -> 4.61 us
  starting transfers between devices: 21.9 us -> 37.6 us
  blocking collectives: 161 us -> 164 us
    all_gather x0 -> x2, blocking collectives: none -> 54.4 us  [gather_early(): lax.all_gather(piece, 'fs', axis=0, tiled=True, axis_index_groups=close)]
    all_to_all x4 -> x3, blocking collectives: 86.3 us -> 35.1 us  [the longest x2 24.9 us: summed_over_peers(): lax.all_to_all(pair.astype(jnp.bfloat16), 'tp', 0, 0, tiled=True, axis_in...]
    ppermute x2, waiting for transfers between devices: 30.4 us -> 0.01 us  [parts_of_all_groups(): behind.append(lax.ppermute(behind[-1], 'grp', up))]
    all_to_all x2 -> x1, waiting for transfers between devices: 27.1 us -> 0.01 us  [from_everyone(): lax.all_to_all(copies, 'tp', 0, 0, tiled=True, axis_index_groups=groups)]
    ppermute x0 -> x4, starting transfers between devices: none -> 25.5 us  [with_partner(): lax.ppermute(x, 'tp', [(k, k + 1 - 2 * (k % CORES)) for k in range(member...]
    all_to_all x2 -> x1, starting transfers between devices: 16.4 us -> 5.27 us  [from_everyone(): lax.all_to_all(copies, 'tp', 0, 0, tiled=True, axis_index_groups=groups)]
    ppermute x0 -> x4, waiting for transfers between devices: none -> 4.55 us  [with_partner(): lax.ppermute(x, 'tp', [(k, k + 1 - 2 * (k % CORES)) for k in range(member...]
  transfers between devices with their start and end apart: 5 -> 8, of which waited for: 3 -> 3; matrix products, arithmetic and copies ran while one was open for 2% -> 3% of each run, Pallas kernels for 1% -> 2%
where the time goes in v1:
time: 244 us; the launch traced here: 243 us
  blocking collectives  164 us (67%)
  starting transfers between devices  37.6 us (15%)
  between operations  13.6 us (6%)
  Pallas kernels  13 us (5%)
  other arithmetic  6.16 us (3%)
  waiting for transfers between devices  4.61 us (2%)
  local copies, waits for them, and re-layouts  4 us (2%)
    all_gather x1, blocking collectives, gather_early(): lax.all_gather(part, 'fs', axis=0, tiled=True, axis_index_groups=strided)  74.9 us
    all_gather x2, blocking collectives, gather_early(): lax.all_gather(piece, 'fs', axis=0, tiled=True, axis_index_groups=close)  54.4 us
    ppermute x4, starting transfers between devices, with_partner(): lax.ppermute(x, 'tp', [(k, k + 1 - 2 * (k % CORES)) for k in range(member...  25.5 us
    all_to_all x2, blocking collectives, summed_over_peers(): lax.all_to_all(pair.astype(jnp.bfloat16), 'tp', 0, 0, tiled=True, axis_in...  24.9 us
    all_to_all x1, blocking collectives, from_everyone(): lax.all_to_all(copies, 'tp', 0, 0, tiled=True, axis_index_groups=groups)  10.2 us
    pallas_call x1, Pallas kernels, feed_forward(): pl.pallas_call(feed_forward_body, out_shape=[jax.ShapeDtypeStruct(tiles[0...  7.81 us
    ppermute x2, starting transfers between devices, parts_of_all_groups(): behind.append(lax.ppermute(behind[-1], 'grp', up))  6.92 us
    all_to_all x1, starting transfers between devices, from_everyone(): lax.all_to_all(copies, 'tp', 0, 0, tiled=True, axis_index_groups=groups)  5.27 us
  transfers between devices with their start and end apart: 8, of which 3 were waited for; matrix products, arithmetic and copies ran while one was open for 3% of the time, Pallas kernels for 2%

profile of v1, /device:TPU:33, one launch (start us, length us, event | category | flops | bytes accessed | tf_op | source)
XLA Modules:
  0.0 243.4 jit_solution(3293968376854660028)
XLA Ops:
  6.6 1.7 pad_maximum_fusion
  8.3 0.8 fusion.1
  9.1 74.9 %all_gather.12 = bf16[256,768]{1,0:T(8,128)(2,1)S(1)} all-gather(bf16[32,768]{1,0:T(8,128)(2,1)S(1)} %fusion.1), channel_id=1, replica_groups={{0,32,64,96,128,160,192,224},{8,40,72,104,136,168,200,232},{16,48,80,11..., dimensions={0}, use_global_device_ids=true | all-gather | bytes 442368 | tf_op jit(solution)/shard_map/all_gather | solution.py:91
  84.0 28.0 %all_gather.14.refs_3_ = bf16[1024,384]{1,0:T(8,128)(2,1)S(1)} all-gather(bf16[256,384]{1,0:T(8,128)(2,1)S(1)} %get-tuple-element.21), channel_id=1, replica_groups={{0,8,16,24},{32,40,48,56},{64,72,80,88},{96,104,112,120},{128,136,144,1..., dimensions={0}, use_global_device_ids=true | all-gather | bytes 983040 | tf_op jit(solution)/shard_map/all_gather | solution.py:97
  112.0 1.7 broadcast_in_dim.18
  113.8 5.3 %all-to-all-start = ((bf16[4,256,256]{2,1,0:T(8,128)(2,1)}), bf16[4,256,256]{2,1,0:T(8,128)(2,1)S(1)}, u32[]{:S(2)}, u32[]{:S(2)}) async-start(bf16[4,256,256]{2,1,0:T(8,128)(2,1)} %broadcast_in_dim.18), calls=%async_computation | async-start | bytes 1048576 | tf_op jit(solution)/shard_map/all_to_all | solution.py:28
  119.0 4.1 %collective-permute-start.1 = (bf16[1024,384]{1,0:T(8,128)(2,1)S(1)}, bf16[1024,384]{1,0:T(8,128)(2,1)S(1)}, u32[]{:S(2)}, u32[]{:S(2)}) collective-permute-start(bf16[1024,384]{1,0:T(8,128)(2,1)S(1)} %all_gather.14.refs_3_), channel_id=1, source_target_pairs={{0,256},{256,0},{1,257},{257,1},{2,258},{258,2},{3,259},{259,3},{4... | collective-permute-start | bytes 2359304 | tf_op jit(solution)/shard_map/ppermute | solution.py:76
  123.1 26.4 %all_gather.13.refs_1_ = bf16[1024,384]{1,0:T(8,128)(2,1)S(1)} all-gather(bf16[256,384]{1,0:T(8,128)(2,1)S(1)} %get-tuple-element.22), channel_id=1, replica_groups={{0,8,16,24},{32,40,48,56},{64,72,80,88},{96,104,112,120},{128,136,144,1..., dimensions={0}, use_global_device_ids=true | all-gather | bytes 983040 | tf_op jit(solution)/shard_map/all_gather | solution.py:97
  149.5 2.8 %collective-permute-start = (bf16[1024,384]{1,0:T(8,128)(2,1)S(1)}, bf16[1024,384]{1,0:T(8,128)(2,1)}, u32[]{:S(2)}, u32[]{:S(2)}) collective-permute-start(bf16[1024,384]{1,0:T(8,128)(2,1)S(1)} %all_gather.13.refs_1_), channel_id=1, source_target_pairs={{0,256},{256,0},{1,257},{257,1},{2,258},{258,2},{3,259},{259,3},{4... | collective-permute-start | bytes 2359304 | tf_op jit(solution)/shard_map/ppermute | solution.py:76
  152.4 9.7 %collective-permute-start.2 = (bf16[4,256,256]{2,1,0:T(8,128)(2,1)S(1)}, bf16[4,256,256]{2,1,0:T(8,128)(2,1)S(1)}, u32[]{:S(2)}, u32[]{:S(2)}) collective-permute-start(bf16[4,256,256]{2,1,0:T(8,128)(2,1)S(1)} %all-to-all-done.refs_5_), channel_id=1, source_target_pairs={{0,1},{1,0},{2,3},{3,2},{4,5},{5,4},{6,7},{7,6},{8,9},{9,8},{10,11... | collective-permute-start | bytes 1572872 | tf_op jit(solution)/shard_map/ppermute | solution.py:22
  162.1 0.8 copy.14.refs_11_
  162.9 0.1 pad_add_fusion.refs_0_
  163.0 0.9 pad_maximum_fusion.1.refs_9_
  163.9 0.7 fusion.2
  164.6 0.7 copy-done
  165.3 0.7 copy-done.2
  166.0 5.2 %recurrent.1 = (bf16[4,256,256]{2,1,0:T(8,128)(2,1)S(1)}, bf16[4,256,256]{2,1,0:T(8,128)(2,1)S(1)}) custom-call(s32[2]{0:T(128)S(1)} %pad_add_fusion.refs_0_, bf16[1024,384]{1,0:T(8,128)(2,1)S(1)} %all_gather.13.refs_1_, bf16[1024,384]{1,0:T(8,128)(2,1)} %collective-permute-done.refs_2_, bf16[1024,384]{1,0:T(8,128)(2,1)S(1)} %all_gather.14.refs_3_, ...), custom_call_target="tpu_custom_call" | custom-call | flops 805306368 | bytes 5242880 | tf_op jit(solution)/shard_map/recurrent/pallas_call | solution.py:188
  171.2 8.8 %collective-permute-start.3 = (bf16[4,256,256]{2,1,0:T(8,128)(2,1)S(1)}, bf16[4,256,256]{2,1,0:T(8,128)(2,1)S(1)}, u32[]{:S(2)}, u32[]{:S(2)}) collective-permute-start(bf16[4,256,256]{2,1,0:T(8,128)(2,1)S(1)} %get-tuple-element.17), channel_id=1, source_target_pairs={{0,1},{1,0},{2,3},{3,2},{4,5},{5,4},{6,7},{7,6},{8,9},{9,8},{10,11... | collective-permute-start | bytes 1572872 | tf_op jit(solution)/shard_map/ppermute | solution.py:22
  180.1 1.5 collective-permute-done.3
  181.6 0.1 add_convert_fusion.1
  181.7 13.2 %all_to_all.20 = bf16[4,256,256]{2,1,0:T(8,128)(2,1)S(1)} all-to-all(bf16[4,256,256]{2,1,0:T(8,128)(2,1)S(1)} %add_convert_fusion.1), channel_id=1, replica_groups={{0,2,4,6},{1,3,5,7},{8,10,12,14},{9,11,13,15},{16,18,20,22},{17,19,21,2..., dimensions={0} | all-to-all | bytes 1048576 | tf_op jit(solution)/shard_map/all_to_all | solution.py:34
  195.0 0.9 add_convert_fusion.3
  196.0 10.2 %all_to_all.21.mine = bf16[4,256,256]{2,1,0:T(8,128)(2,1)S(1)} all-to-all(bf16[4,256,256]{2,1,0:T(8,128)(2,1)S(1)} %broadcast_in_dim.22), channel_id=1, replica_groups={{0,2,4,6},{1,3,5,7},{8,10,12,14},{9,11,13,15},{16,18,20,22},{17,19,21,2..., dimensions={0} | all-to-all | bytes 1048576 | tf_op jit(solution)/shard_map/all_to_all | solution.py:28
  206.2 4.6 %collective-permute-start.4 = (bf16[4,256,256]{2,1,0:T(8,128)(2,1)S(1)}, bf16[4,256,256]{2,1,0:T(8,128)(2,1)S(1)}, u32[]{:S(2)}, u32[]{:S(2)}) collective-permute-start(bf16[4,256,256]{2,1,0:T(8,128)(2,1)S(1)} %all_to_all.21.mine), channel_id=1, source_target_pairs={{0,1},{1,0},{2,3},{3,2},{4,5},{5,4},{6,7},{7,6},{8,9},{9,8},{10,11... | collective-permute-start | bytes 1572872 | tf_op jit(solution)/shard_map/ppermute | solution.py:22
  210.8 1.5 collective-permute-done.4.other
  212.4 7.8 %feed_forward.1 = (bf16[4,256,256]{2,1,0:T(8,128)(2,1)S(1)}, bf16[4,256,256]{2,1,0:T(8,128)(2,1)S(1)}) custom-call(s32[1]{0:T(128)} %bitcast.2.core_ref, bf16[4,256,256]{2,1,0:T(8,128)(2,1)S(1)} %all_to_all.21.mine, bf16[4,256,256]{2,1,0:T(8,128)(2,1)S(1)} %collective-permute-done.4.other, f32[1,2048]{1,0:T(1,128)S(1)} %bitcast.9, ...), custom_call_target="tpu_custom_call" | custom-call | flops 2147483648 | bytes 10485760 | tf_op jit(solution)/shard_map/feed_forward/pallas_call | solution.py:260
  220.2 2.3 collective-permute-start.5
  222.5 1.5 collective-permute-done.5
  224.0 0.1 add_convert_fusion
  224.1 11.6 %all_to_all.22 = bf16[4,256,256]{2,1,0:T(8,128)(2,1)S(1)} all-to-all(bf16[4,256,256]{2,1,0:T(8,128)(2,1)S(1)} %add_convert_fusion), channel_id=1, replica_groups={{0,2,4,6},{1,3,5,7},{8,10,12,14},{9,11,13,15},{16,18,20,22},{17,19,21,2..., dimensions={0} | all-to-all | bytes 1048576 | tf_op jit(solution)/shard_map/all_to_all | solution.py:34
  235.8 0.1 convert_reduce_fusion
  235.9 0.7 add_convert_fusion.2
  (14 shorter events, 0.2 us)
Async XLA Ops:
  6.5 205.8 %copy-start.1 = (f32[2048]{0:T(1024)S(1)}, f32[2048]{0:T(1024)}, u32[]{:S(2)}) copy-start(f32[2048]{0:T(1024)} %param.15) | copy-start | bytes 24580
  6.5 205.8 %all-gather.2.cloned.1.call-start = ((), (), s32[]{:S(2)}) async-start(), calls=%async_computation.4 | async-start | bytes 8650752 | tf_op jit(solution)/shard_map/all_gather | solution.py:305
  113.8 38.6 %all-to-all-start = ((bf16[4,256,256]{2,1,0:T(8,128)(2,1)}), bf16[4,256,256]{2,1,0:T(8,128)(2,1)S(1)}, u32[]{:S(2)}, u32[]{:S(2)}) async-start(bf16[4,256,256]{2,1,0:T(8,128)(2,1)} %broadcast_in_dim.18), calls=%async_computation | async-start | bytes 1048576 | tf_op jit(solution)/shard_map/all_to_all | solution.py:28
  119.0 45.6 %collective-permute-start.1 = (bf16[1024,384]{1,0:T(8,128)(2,1)S(1)}, bf16[1024,384]{1,0:T(8,128)(2,1)S(1)}, u32[]{:S(2)}, u32[]{:S(2)}) collective-permute-start(bf16[1024,384]{1,0:T(8,128)(2,1)S(1)} %all_gather.14.refs_3_), channel_id=1, source_target_pairs={{0,256},{256,0},{1,257},{257,1},{2,258},{258,2},{3,259},{259,3},{4... | collective-permute-start | bytes 2359304 | tf_op jit(solution)/shard_map/ppermute | solution.py:76
  149.5 15.1 %collective-permute-start = (bf16[1024,384]{1,0:T(8,128)(2,1)S(1)}, bf16[1024,384]{1,0:T(8,128)(2,1)}, u32[]{:S(2)}, u32[]{:S(2)}) collective-permute-start(bf16[1024,384]{1,0:T(8,128)(2,1)S(1)} %all_gather.13.refs_1_), channel_id=1, source_target_pairs={{0,256},{256,0},{1,257},{257,1},{2,258},{258,2},{3,259},{259,3},{4... | collective-permute-start | bytes 2359304 | tf_op jit(solution)/shard_map/ppermute | solution.py:76
  152.4 12.2 %collective-permute-start.2 = (bf16[4,256,256]{2,1,0:T(8,128)(2,1)S(1)}, bf16[4,256,256]{2,1,0:T(8,128)(2,1)S(1)}, u32[]{:S(2)}, u32[]{:S(2)}) collective-permute-start(bf16[4,256,256]{2,1,0:T(8,128)(2,1)S(1)} %all-to-all-done.refs_5_), channel_id=1, source_target_pairs={{0,1},{1,0},{2,3},{3,2},{4,5},{5,4},{6,7},{7,6},{8,9},{9,8},{10,11... | collective-permute-start | bytes 1572872 | tf_op jit(solution)/shard_map/ppermute | solution.py:22
  164.6 0.7 copy-start
  165.3 0.7 copy-start.2
  171.2 10.4 %collective-permute-start.3 = (bf16[4,256,256]{2,1,0:T(8,128)(2,1)S(1)}, bf16[4,256,256]{2,1,0:T(8,128)(2,1)S(1)}, u32[]{:S(2)}, u32[]{:S(2)}) collective-permute-start(bf16[4,256,256]{2,1,0:T(8,128)(2,1)S(1)} %get-tuple-element.17), channel_id=1, source_target_pairs={{0,1},{1,0},{2,3},{3,2},{4,5},{5,4},{6,7},{7,6},{8,9},{9,8},{10,11... | collective-permute-start | bytes 1572872 | tf_op jit(solution)/shard_map/ppermute | solution.py:22
  206.2 6.1 %collective-permute-start.4 = (bf16[4,256,256]{2,1,0:T(8,128)(2,1)S(1)}, bf16[4,256,256]{2,1,0:T(8,128)(2,1)S(1)}, u32[]{:S(2)}, u32[]{:S(2)}) collective-permute-start(bf16[4,256,256]{2,1,0:T(8,128)(2,1)S(1)} %all_to_all.21.mine), channel_id=1, source_target_pairs={{0,1},{1,0},{2,3},{3,2},{4,5},{5,4},{6,7},{7,6},{8,9},{9,8},{10,11... | collective-permute-start | bytes 1572872 | tf_op jit(solution)/shard_map/ppermute | solution.py:22
  220.2 3.8 %collective-permute-start.5 = (bf16[4,256,256]{2,1,0:T(8,128)(2,1)S(1)}, bf16[4,256,256]{2,1,0:T(8,128)(2,1)S(1)}, u32[]{:S(2)}, u32[]{:S(2)}) collective-permute-start(bf16[4,256,256]{2,1,0:T(8,128)(2,1)S(1)} %get-tuple-element.20), channel_id=1, source_target_pairs={{0,1},{1,0},{2,3},{3,2},{4,5},{5,4},{6,7},{7,6},{8,9},{9,8},{10,11... | collective-permute-start | bytes 1572872 | tf_op jit(solution)/shard_map/ppermute | solution.py:22
Sparse Core Ops, SparseCore 0:
  9.4 184.0 all-gather.1

commit v2 on v1

--- a/solution.py
+++ b/solution.py
@@ -42,9 +42,7 @@
     blocks = CORES * half
 
     def tile(k):
-        first = mine[k // CORES].astype(jnp.float32)
-        second = other[k // CORES].astype(jnp.float32)
-        return jnp.where(core == k % CORES, first, second)
+        return (mine if core == k % CORES else other)[k // CORES].astype(jnp.float32)
 
     squares = jnp.zeros((length, 1), jnp.float32)
     for k in range(blocks):
@@ -57,13 +55,15 @@
 
 
 def put(core, k, value, keep, give):
-    @pl.when(core == k % CORES)
-    def _():
-        keep[k // CORES] = value
-
-    @pl.when(core != k % CORES)
-    def _():
-        give[k // CORES] = value
+    (keep if core == k % CORES else give)[k // CORES] = value
+
+
+def on_each_core(core, body):
+    for c in range(CORES):
+
+        @pl.when(core == c)
+        def _(c=c):
+            body(c)
 
 
 def parts_of_all_groups(mine):
@@ -108,12 +108,14 @@
 
 def recurrent_body(groups, pieces, runs, me_ref, *refs):
     parts = refs[: pieces * groups]
-    (mine, other, gain, taps, maps, rate, extra, keep, give, normed, weights) = refs[
-        pieces * groups :
-    ]
+    mine, other, *small = refs[pieces * groups : pieces * groups + 8]
+    keep, give, normed, weights, *held, landed = refs[pieces * groups + 8 :]
+    copies = [pltpu.make_async_copy(s, h, landed.at[k]) for k, (s, h) in enumerate(zip(small, held))]
+    for copy in copies:
+        copy.start()
+    gain, taps, decay_map, input_map, base, extra = held
     half, length, block = mine.shape
     blocks = CORES * half
-    core = me_ref[1]
     width = taps.shape[1]
     each = parts[0].shape[0] // (RUN * runs)
     wide = parts[0].shape[1]
@@ -127,7 +129,9 @@
                     weights[pl.ds(to, each), piece * wide : (piece + 1) * wide] = parts[
                         piece * groups + behind
                     ][start : start + each, :]
-    norm_rows(core, mine, other, gain, normed)
+    for copy in copies:
+        copy.wait()
+    on_each_core(me_ref[1], lambda core: norm_rows(core, mine, other, gain, normed))
     recur = jnp.dot(normed[...], weights[:, :width], preferred_element_type=jnp.float32)
     gate_pre = jnp.dot(
         normed[...], weights[:, width : 2 * width], preferred_element_type=jnp.float32
@@ -141,17 +145,21 @@
             jnp.float32
         )
     conv_rows = conv_sum.astype(jnp.bfloat16)
-    count = maps.shape[0] // 2
+    count = decay_map.shape[0]
     size = width // count
     recur_gate = []
     input_rate = []
     for k in range(count):
         x = conv_rows[:, k * size : (k + 1) * size]
-        recur_gate.append(jnp.dot(x, maps[k], preferred_element_type=jnp.float32))
-        input_rate.append(jnp.dot(x, maps[count + k], preferred_element_type=jnp.float32))
+        recur_gate.append(jnp.dot(x, decay_map[k], preferred_element_type=jnp.float32))
+        input_rate.append(jnp.dot(x, input_map[k], preferred_element_type=jnp.float32))
     recur_gate = jax.nn.sigmoid(jnp.concatenate(recur_gate, axis=1))
     input_rate = jax.nn.sigmoid(jnp.concatenate(input_rate, axis=1))
-    log_decay = rate[...] * recur_gate + extra[...]
+    x = -base[...]
+    softplus = jnp.maximum(x, 0.0) + jnp.log1p(jnp.exp(-jnp.abs(x)))
+    columns = jnp.broadcast_to(extra[...], (128, length)).T
+    columns = jnp.concatenate([columns] * (width // 128), axis=1)
+    log_decay = -8.0 * softplus * recur_gate + columns
     decay = jnp.exp(log_decay)
     u = -log_decay
     small = 2.0 * u * (1.0 - u * (1.0 - u * (2.0 / 3.0 - u * (1.0 / 3.0 - u * (2.0 / 15.0)))))
@@ -164,14 +172,18 @@
             decay = decay * shifted(decay, by, 1.0)
         by *= 2
     mixed = (hidden * gate).astype(jnp.bfloat16)
-    for k in range(blocks):
-        product = lax.dot_general(
-            mixed,
-            weights[k * block : (k + 1) * block, 2 * width : 3 * width],
-            (((1,), (1,)), ((), ())),
-            preferred_element_type=jnp.float32,
-        )
-        put(core, k, product.astype(jnp.bfloat16), keep, give)
+
+    def finish(core):
+        for k in range(blocks):
+            product = lax.dot_general(
+                mixed,
+                weights[k * block : (k + 1) * block, 2 * width : 3 * width],
+                (((1,), (1,)), ((), ())),
+                preferred_element_type=jnp.float32,
+            )
+            put(core, k, product.astype(jnp.bfloat16), keep, give)
+
+    on_each_core(me_ref[1], finish)
 
 
 def recurrent_block(tiles, parts, gain, taps, decay_gate, input_gate, base, extra):
@@ -179,7 +191,7 @@
     pieces = len(parts)
     runs = lax.axis_size("fs") // RUN
     place = jnp.stack([lax.axis_index("grp"), lax.axis_index("tp") % CORES]).astype(jnp.int32)
-    rate = (-8.0 * jax.nn.softplus(-base))[None, :]
+    small = [gain[None, :], taps, decay_gate, input_gate, base[None, :], extra[None, :]]
     flat = [p for piece in parts for p in piece]
     half, length, block = tiles[0].shape
     vmem = pl.BlockSpec(memory_space=pltpu.VMEM)
@@ -188,11 +200,14 @@
     return pl.pallas_call(
         lambda *refs: recurrent_body(groups, pieces, runs, *refs),
         out_shape=[jax.ShapeDtypeStruct(tiles[0].shape, jnp.bfloat16)] * 2,
-        in_specs=[pl.BlockSpec(memory_space=pltpu.SMEM)] + [vmem] * (len(flat) + 7),
+        in_specs=[pl.BlockSpec(memory_space=pltpu.SMEM)] + [vmem] * (len(flat) + 2)
+        + [pl.BlockSpec(memory_space=pltpu.HBM)] * len(small),
         out_specs=[vmem] * 2,
         scratch_shapes=[
             pltpu.VMEM((length, features), jnp.bfloat16),
             pltpu.VMEM((features, cols), jnp.bfloat16),
+            *[pltpu.VMEM(s.shape, s.dtype) for s in small],
+            pltpu.SemaphoreType.DMA((len(small),)),
         ],
         cost_estimate=pl.CostEstimate(
             flops=2 * length * features * cols,
@@ -205,11 +220,7 @@
         place,
         *flat,
         *tiles,
-        gain[None, :],
-        taps,
-        jnp.concatenate([decay_gate, input_gate]),
-        rate,
-        extra[:, None],
+        *[pltpu.with_memory_space_constraint(s, pltpu.HBM) for s in small],
     )
 
 
@@ -218,7 +229,6 @@
 ):
     half, _, block = mine.shape
     blocks = CORES * half
-    core = core_ref[0]
     hidden = squared.shape[1]
     chunks = hidden // CHUNK
     ups = [
@@ -233,21 +243,26 @@
     ]
     for copy in ups + downs:
         copy.start()
-    norm_rows(core, mine, other, gain, normed)
+    on_each_core(core_ref[0], lambda core: norm_rows(core, mine, other, gain, normed))
     for k in range(chunks):
         ups[k].wait()
         upward = jnp.dot(normed[...], up[k], preferred_element_type=jnp.float32)
         positive = jnp.maximum(upward, 0.0)
         squared[:, k * CHUNK : (k + 1) * CHUNK] = (positive * positive).astype(jnp.bfloat16)
-    for k in range(blocks):
-        downs[k].wait()
-        product = lax.dot_general(
-            squared[...],
-            down[k],
-            (((1,), (1,)), ((), ())),
-            preferred_element_type=jnp.float32,
-        )
-        put(core, k, product.astype(jnp.bfloat16), keep, give)
+    for copy in downs:
+        copy.wait()
+
+    def finish(core):
+        for k in range(blocks):
+            product = lax.dot_general(
+                squared[...],
+                down[k],
+                (((1,), (1,)), ((), ())),
+                preferred_element_type=jnp.float32,
+            )
+            put(core, k, product.astype(jnp.bfloat16), keep, give)
+
+    on_each_core(core_ref[0], finish)
 
 
 def feed_forward(tiles, gain, weights):

time: 244 us -> 239 us (0.980)
  Pallas kernels: 13 us -> 10.2 us
  other arithmetic: 6.16 us -> 3.7 us
  transfers between devices with their start and end apart: 8 -> 8, of which waited for: 3 -> 5; matrix products, arithmetic and copies ran while one was open for 3% -> 1% of each run, Pallas kernels for 2% -> 2%
where the time goes in v2:
time: 239 us; the launch traced here: 238 us
  blocking collectives  165 us (69%)
  starting transfers between devices  38 us (16%)
  between operations  13.5 us (6%)
  Pallas kernels  10.2 us (4%)
  waiting for transfers between devices  6.03 us (3%)
  other arithmetic  3.7 us (2%)
    all_gather x1, blocking collectives, gather_early(): lax.all_gather(part, 'fs', axis=0, tiled=True, axis_index_groups=strided)  75.1 us
    all_gather x2, blocking collectives, gather_early(): lax.all_gather(piece, 'fs', axis=0, tiled=True, axis_index_groups=close)  55.3 us
    ppermute x4, starting transfers between devices, with_partner(): lax.ppermute(x, 'tp', [(k, k + 1 - 2 * (k % CORES)) for k in range(member...  27.4 us
    all_to_all x2, blocking collectives, summed_over_peers(): lax.all_to_all(pair.astype(jnp.bfloat16), 'tp', 0, 0, tiled=True, axis_in...  24.4 us
    all_to_all x1, blocking collectives, from_everyone(): lax.all_to_all(copies, 'tp', 0, 0, tiled=True, axis_index_groups=groups)  10.2 us
    ppermute x2, starting transfers between devices, parts_of_all_groups(): behind.append(lax.ppermute(behind[-1], 'grp', up))  6.02 us
    pallas_call x1, Pallas kernels, feed_forward(): pl.pallas_call(feed_forward_body, out_shape=[jax.ShapeDtypeStruct(tiles[0...  5.39 us
    ppermute x4, waiting for transfers between devices, with_partner(): lax.ppermute(x, 'tp', [(k, k + 1 - 2 * (k % CORES)) for k in range(member...  4.83 us
  transfers between devices with their start and end apart: 8, of which 5 were waited for; matrix products, arithmetic and copies ran while one was open for 1% of the time, Pallas kernels for 2%

profile of v2, /device:TPU:33, one launch (start us, length us, event | category | flops | bytes accessed | tf_op | source)
XLA Modules:
  0.0 238.3 jit_solution(16222355438939546849)
XLA Ops:
  6.6 1.7 pad_maximum_fusion
  8.3 0.1 all-gather.2.cloned.1.call-update
  8.3 0.8 fusion.1
  9.1 75.1 %all_gather.12 = bf16[256,768]{1,0:T(8,128)(2,1)S(1)} all-gather(bf16[32,768]{1,0:T(8,128)(2,1)S(1)} %fusion.1), channel_id=1, replica_groups={{0,32,64,96,128,160,192,224},{8,40,72,104,136,168,200,232},{16,48,80,11..., dimensions={0}, use_global_device_ids=true | all-gather | bytes 442368 | tf_op jit(solution)/shard_map/all_gather | solution.py:91
  84.2 27.9 %all_gather.14.refs_3_ = bf16[1024,384]{1,0:T(8,128)(2,1)S(1)} all-gather(bf16[256,384]{1,0:T(8,128)(2,1)S(1)} %get-tuple-element.21), channel_id=1, replica_groups={{0,8,16,24},{32,40,48,56},{64,72,80,88},{96,104,112,120},{128,136,144,1..., dimensions={0}, use_global_device_ids=true | all-gather | bytes 983040 | tf_op jit(solution)/shard_map/all_gather | solution.py:97
  112.1 1.7 broadcast_in_dim.18
  113.8 4.6 %all-to-all-start = ((bf16[4,256,256]{2,1,0:T(8,128)(2,1)}), bf16[4,256,256]{2,1,0:T(8,128)(2,1)S(1)}, u32[]{:S(2)}, u32[]{:S(2)}) async-start(bf16[4,256,256]{2,1,0:T(8,128)(2,1)} %broadcast_in_dim.18), calls=%async_computation | async-start | bytes 1048576 | tf_op jit(solution)/shard_map/all_to_all | solution.py:28
  118.5 4.1 %collective-permute-start.1 = (bf16[1024,384]{1,0:T(8,128)(2,1)S(1)}, bf16[1024,384]{1,0:T(8,128)(2,1)S(1)}, u32[]{:S(2)}, u32[]{:S(2)}) collective-permute-start(bf16[1024,384]{1,0:T(8,128)(2,1)S(1)} %all_gather.14.refs_3_), channel_id=1, source_target_pairs={{0,256},{256,0},{1,257},{257,1},{2,258},{258,2},{3,259},{259,3},{4... | collective-permute-start | bytes 2359304 | tf_op jit(solution)/shard_map/ppermute | solution.py:76
  122.6 27.5 %all_gather.13.refs_1_ = bf16[1024,384]{1,0:T(8,128)(2,1)S(1)} all-gather(bf16[256,384]{1,0:T(8,128)(2,1)S(1)} %get-tuple-element.22), channel_id=1, replica_groups={{0,8,16,24},{32,40,48,56},{64,72,80,88},{96,104,112,120},{128,136,144,1..., dimensions={0}, use_global_device_ids=true | all-gather | bytes 983040 | tf_op jit(solution)/shard_map/all_gather | solution.py:97
  150.0 1.9 collective-permute-start
  152.0 0.0 all-to-all-done.refs_5_
  152.0 10.0 %collective-permute-start.2 = (bf16[4,256,256]{2,1,0:T(8,128)(2,1)S(1)}, bf16[4,256,256]{2,1,0:T(8,128)(2,1)S(1)}, u32[]{:S(2)}, u32[]{:S(2)}) collective-permute-start(bf16[4,256,256]{2,1,0:T(8,128)(2,1)S(1)} %all-to-all-done.refs_5_), channel_id=1, source_target_pairs={{0,1},{1,0},{2,3},{3,2},{4,5},{5,4},{6,7},{7,6},{8,9},{9,8},{10,11... | collective-permute-start | bytes 1572872 | tf_op jit(solution)/shard_map/ppermute | solution.py:22
  162.0 0.1 pad_add_fusion.refs_0_
  162.1 0.0 collective-permute-done.1.refs_4_
  162.1 1.1 collective-permute-done.refs_2_
  163.2 0.3 collective-permute-done.2.refs_6_
  163.5 4.8 %recurrent.1 = (bf16[4,256,256]{2,1,0:T(8,128)(2,1)S(1)}, bf16[4,256,256]{2,1,0:T(8,128)(2,1)S(1)}) custom-call(s32[2]{0:T(128)S(1)} %pad_add_fusion.refs_0_, bf16[1024,384]{1,0:T(8,128)(2,1)S(1)} %all_gather.13.refs_1_, bf16[1024,384]{1,0:T(8,128)(2,1)} %collective-permute-done.refs_2_, bf16[1024,384]{1,0:T(8,128)(2,1)S(1)} %all_gather.14.refs_3_, ...), custom_call_target="tpu_custom_call" | custom-call | flops 805306368 | bytes 5242880 | tf_op jit(solution)/shard_map/recurrent/pallas_call | solution.py:200
  168.3 10.5 %collective-permute-start.3 = (bf16[4,256,256]{2,1,0:T(8,128)(2,1)S(1)}, bf16[4,256,256]{2,1,0:T(8,128)(2,1)S(1)}, u32[]{:S(2)}, u32[]{:S(2)}) collective-permute-start(bf16[4,256,256]{2,1,0:T(8,128)(2,1)S(1)} %get-tuple-element.17), channel_id=1, source_target_pairs={{0,1},{1,0},{2,3},{3,2},{4,5},{5,4},{6,7},{7,6},{8,9},{9,8},{10,11... | collective-permute-start | bytes 1572872 | tf_op jit(solution)/shard_map/ppermute | solution.py:22
  178.8 1.5 collective-permute-done.3
  180.3 0.1 add_convert_fusion.1
  180.4 12.7 %all_to_all.20 = bf16[4,256,256]{2,1,0:T(8,128)(2,1)S(1)} all-to-all(bf16[4,256,256]{2,1,0:T(8,128)(2,1)S(1)} %add_convert_fusion.1), channel_id=1, replica_groups={{0,2,4,6},{1,3,5,7},{8,10,12,14},{9,11,13,15},{16,18,20,22},{17,19,21,2..., dimensions={0} | all-to-all | bytes 1048576 | tf_op jit(solution)/shard_map/all_to_all | solution.py:34
  193.2 0.1 convert_reduce_fusion.1
  193.3 10.2 %all_to_all.21.mine = bf16[4,256,256]{2,1,0:T(8,128)(2,1)S(1)} all-to-all(bf16[4,256,256]{2,1,0:T(8,128)(2,1)S(1)} %broadcast_in_dim.22), channel_id=1, replica_groups={{0,2,4,6},{1,3,5,7},{8,10,12,14},{9,11,13,15},{16,18,20,22},{17,19,21,2..., dimensions={0} | all-to-all | bytes 1048576 | tf_op jit(solution)/shard_map/all_to_all | solution.py:28
  203.5 4.6 %collective-permute-start.4 = (bf16[4,256,256]{2,1,0:T(8,128)(2,1)S(1)}, bf16[4,256,256]{2,1,0:T(8,128)(2,1)S(1)}, u32[]{:S(2)}, u32[]{:S(2)}) collective-permute-start(bf16[4,256,256]{2,1,0:T(8,128)(2,1)S(1)} %all_to_all.21.mine), channel_id=1, source_target_pairs={{0,1},{1,0},{2,3},{3,2},{4,5},{5,4},{6,7},{7,6},{8,9},{9,8},{10,11... | collective-permute-start | bytes 1572872 | tf_op jit(solution)/shard_map/ppermute | solution.py:22
  208.1 1.5 collective-permute-done.4.other
  209.6 5.4 %feed_forward.1 = (bf16[4,256,256]{2,1,0:T(8,128)(2,1)S(1)}, bf16[4,256,256]{2,1,0:T(8,128)(2,1)S(1)}) custom-call(s32[1]{0:T(128)} %bitcast.2.core_ref, bf16[4,256,256]{2,1,0:T(8,128)(2,1)S(1)} %all_to_all.21.mine, bf16[4,256,256]{2,1,0:T(8,128)(2,1)S(1)} %collective-permute-done.4.other, f32[1,2048]{1,0:T(1,128)S(1)} %bitcast.8, ...), custom_call_target="tpu_custom_call" | custom-call | flops 2147483648 | bytes 10485760 | tf_op jit(solution)/shard_map/feed_forward/pallas_call | solution.py:275
  215.0 2.3 collective-permute-start.5
  217.4 1.5 collective-permute-done.5
  218.9 0.1 add_convert_fusion
  219.0 11.6 %all_to_all.22 = bf16[4,256,256]{2,1,0:T(8,128)(2,1)S(1)} all-to-all(bf16[4,256,256]{2,1,0:T(8,128)(2,1)S(1)} %add_convert_fusion), channel_id=1, replica_groups={{0,2,4,6},{1,3,5,7},{8,10,12,14},{9,11,13,15},{16,18,20,22},{17,19,21,2..., dimensions={0} | all-to-all | bytes 1048576 | tf_op jit(solution)/shard_map/all_to_all | solution.py:34
  230.7 0.1 convert_reduce_fusion
  230.7 0.7 add_convert_fusion.2
  (9 shorter events, 0.1 us)
Async XLA Ops:
  6.5 186.7 %copy-start.1 = (bf16[256,256]{1,0:T(8,128)(2,1)S(1)}, bf16[256,256]{1,0:T(8,128)(2,1)}, u32[]{:S(2)}) copy-start(bf16[256,256]{1,0:T(8,128)(2,1)} %param.13) | copy-start | bytes 393220
  6.5 203.1 %copy-start = (f32[2048]{0:T(1024)S(1)}, f32[2048]{0:T(1024)}, u32[]{:S(2)}) copy-start(f32[2048]{0:T(1024)} %param.15) | copy-start | bytes 24580
  6.6 203.1 %all-gather.2.cloned.1.call-start = ((), (), s32[]{:S(2)}) async-start(), calls=%async_computation.4 | async-start | bytes 8650752 | tf_op jit(solution)/shard_map/all_gather | solution.py:320
  113.8 38.2 %all-to-all-start = ((bf16[4,256,256]{2,1,0:T(8,128)(2,1)}), bf16[4,256,256]{2,1,0:T(8,128)(2,1)S(1)}, u32[]{:S(2)}, u32[]{:S(2)}) async-start(bf16[4,256,256]{2,1,0:T(8,128)(2,1)} %broadcast_in_dim.18), calls=%async_computation | async-start | bytes 1048576 | tf_op jit(solution)/shard_map/all_to_all | solution.py:28
  118.5 43.6 %collective-permute-start.1 = (bf16[1024,384]{1,0:T(8,128)(2,1)S(1)}, bf16[1024,384]{1,0:T(8,128)(2,1)S(1)}, u32[]{:S(2)}, u32[]{:S(2)}) collective-permute-start(bf16[1024,384]{1,0:T(8,128)(2,1)S(1)} %all_gather.14.refs_3_), channel_id=1, source_target_pairs={{0,256},{256,0},{1,257},{257,1},{2,258},{258,2},{3,259},{259,3},{4... | collective-permute-start | bytes 2359304 | tf_op jit(solution)/shard_map/ppermute | solution.py:76
  150.0 13.2 %collective-permute-start = (bf16[1024,384]{1,0:T(8,128)(2,1)S(1)}, bf16[1024,384]{1,0:T(8,128)(2,1)}, u32[]{:S(2)}, u32[]{:S(2)}) collective-permute-start(bf16[1024,384]{1,0:T(8,128)(2,1)S(1)} %all_gather.13.refs_1_), channel_id=1, source_target_pairs={{0,256},{256,0},{1,257},{257,1},{2,258},{258,2},{3,259},{259,3},{4... | collective-permute-start | bytes 2359304 | tf_op jit(solution)/shard_map/ppermute | solution.py:76
  152.0 11.5 %collective-permute-start.2 = (bf16[4,256,256]{2,1,0:T(8,128)(2,1)S(1)}, bf16[4,256,256]{2,1,0:T(8,128)(2,1)S(1)}, u32[]{:S(2)}, u32[]{:S(2)}) collective-permute-start(bf16[4,256,256]{2,1,0:T(8,128)(2,1)S(1)} %all-to-all-done.refs_5_), channel_id=1, source_target_pairs={{0,1},{1,0},{2,3},{3,2},{4,5},{5,4},{6,7},{7,6},{8,9},{9,8},{10,11... | collective-permute-start | bytes 1572872 | tf_op jit(solution)/shard_map/ppermute | solution.py:22
  168.3 12.0 %collective-permute-start.3 = (bf16[4,256,256]{2,1,0:T(8,128)(2,1)S(1)}, bf16[4,256,256]{2,1,0:T(8,128)(2,1)S(1)}, u32[]{:S(2)}, u32[]{:S(2)}) collective-permute-start(bf16[4,256,256]{2,1,0:T(8,128)(2,1)S(1)} %get-tuple-element.17), channel_id=1, source_target_pairs={{0,1},{1,0},{2,3},{3,2},{4,5},{5,4},{6,7},{7,6},{8,9},{9,8},{10,11... | collective-permute-start | bytes 1572872 | tf_op jit(solution)/shard_map/ppermute | solution.py:22
  203.5 6.1 %collective-permute-start.4 = (bf16[4,256,256]{2,1,0:T(8,128)(2,1)S(1)}, bf16[4,256,256]{2,1,0:T(8,128)(2,1)S(1)}, u32[]{:S(2)}, u32[]{:S(2)}) collective-permute-start(bf16[4,256,256]{2,1,0:T(8,128)(2,1)S(1)} %all_to_all.21.mine), channel_id=1, source_target_pairs={{0,1},{1,0},{2,3},{3,2},{4,5},{5,4},{6,7},{7,6},{8,9},{9,8},{10,11... | collective-permute-start | bytes 1572872 | tf_op jit(solution)/shard_map/ppermute | solution.py:22
  215.0 3.8 %collective-permute-start.5 = (bf16[4,256,256]{2,1,0:T(8,128)(2,1)S(1)}, bf16[4,256,256]{2,1,0:T(8,128)(2,1)S(1)}, u32[]{:S(2)}, u32[]{:S(2)}) collective-permute-start(bf16[4,256,256]{2,1,0:T(8,128)(2,1)S(1)} %get-tuple-element.20), channel_id=1, source_target_pairs={{0,1},{1,0},{2,3},{3,2},{4,5},{5,4},{6,7},{7,6},{8,9},{9,8},{10,11... | collective-permute-start | bytes 1572872 | tf_op jit(solution)/shard_map/ppermute | solution.py:22
Sparse Core Ops, SparseCore 0:
  9.4 183.7 all-gather.1

commit v3 on v2

--- a/solution.py
+++ b/solution.py
@@ -6,7 +6,7 @@
 from jax.sharding import PartitionSpec as P
 
 
-RUN = 4
+RUN = 2
 CORES = 2
 CHUNK = 256
 PIECES = 2
@@ -87,18 +87,21 @@
     runs = ring // RUN
     part = lax.dynamic_slice_in_dim(shard, me * (rows // groups), rows // groups, 0)
     strided = [[k + RUN * j for j in range(runs)] for k in range(RUN)]
-    close = [[RUN * m + k for k in range(RUN)] for m in range(runs)]
+    neighbour = [(k, k + 1 - 2 * (k % RUN)) for k in range(ring)]
     level = lax.all_gather(part, "fs", axis=0, tiled=True, axis_index_groups=strided)
-    pieces = PIECES
-    wide = cols // pieces
-    done = []
-    for k in range(pieces):
-        piece = level[:, k * wide : (k + 1) * wide]
-        got = lax.all_gather(piece, "fs", axis=0, tiled=True, axis_index_groups=close)
-        if k == pieces - 1:
-            got, waiting = lax.optimization_barrier((got, waiting))
-        done.append(parts_of_all_groups(got))
-    return done, waiting
+    wide = cols // PIECES
+    own = [level[:, k * wide : (k + 1) * wide] for k in range(PIECES)]
+    near = []
+    for k in range(PIECES):
+        near.append(lax.ppermute(own[k], "fs", neighbour))
+    far = [parts_of_all_groups(own[k]) for k in range(PIECES)]
+    beyond = []
+    for k in range(PIECES):
+        if groups == 2 and k == PIECES - 1:
+            beyond.append([near[k], lax.ppermute(far[k][1], "fs", neighbour)])
+        else:
+            beyond.append(parts_of_all_groups(near[k]))
+    return [far[k] + beyond[k] for k in range(PIECES)], waiting
 
 
 def shifted(x, by, fill):
@@ -107,9 +110,10 @@
 
 
 def recurrent_body(groups, pieces, runs, me_ref, *refs):
-    parts = refs[: pieces * groups]
-    mine, other, *small = refs[pieces * groups : pieces * groups + 8]
-    keep, give, normed, weights, *held, landed = refs[pieces * groups + 8 :]
+    taken = pieces * RUN * groups
+    parts = refs[:taken]
+    mine, other, *small = refs[taken : taken + 8]
+    keep, give, normed, weights, *held, landed = refs[taken + 8 :]
     copies = [pltpu.make_async_copy(s, h, landed.at[k]) for k, (s, h) in enumerate(zip(small, held))]
     for copy in copies:
         copy.start()
@@ -117,18 +121,18 @@
     half, length, block = mine.shape
     blocks = CORES * half
     width = taps.shape[1]
-    each = parts[0].shape[0] // (RUN * runs)
+    each = parts[0].shape[0] // runs
     wide = parts[0].shape[1]
     for behind in range(groups):
         place = lax.rem(me_ref[0] + groups - behind, groups) * each
-        for near in range(RUN):
+        for side in range(RUN):
+            near = lax.rem(me_ref[2] + side, RUN) * groups * each
             for far in range(runs):
-                to = pl.multiple_of((far * RUN + near) * groups * each + place, each)
-                start = (near * runs + far) * each
+                to = pl.multiple_of(far * RUN * groups * each + near + place, each)
                 for piece in range(pieces):
                     weights[pl.ds(to, each), piece * wide : (piece + 1) * wide] = parts[
-                        piece * groups + behind
-                    ][start : start + each, :]
+                        (piece * RUN + side) * groups + behind
+                    ][far * each : (far + 1) * each, :]
     for copy in copies:
         copy.wait()
     on_each_core(me_ref[1], lambda core: norm_rows(core, mine, other, gain, normed))
@@ -187,10 +191,12 @@
 
 
 def recurrent_block(tiles, parts, gain, taps, decay_gate, input_gate, base, extra):
-    groups = len(parts[0])
+    groups = len(parts[0]) // RUN
     pieces = len(parts)
     runs = lax.axis_size("fs") // RUN
-    place = jnp.stack([lax.axis_index("grp"), lax.axis_index("tp") % CORES]).astype(jnp.int32)
+    place = jnp.stack(
+        [lax.axis_index("grp"), lax.axis_index("tp") % CORES, lax.axis_index("fs") % RUN]
+    ).astype(jnp.int32)
     small = [gain[None, :], taps, decay_gate, input_gate, base[None, :], extra[None, :]]
     flat = [p for piece in parts for p in piece]
     half, length, block = tiles[0].shape

time: 239 us -> 238 us (level)
  blocking collectives: 165 us -> 115 us
  waiting for transfers between devices: 6.03 us -> 35.7 us
  starting transfers between devices: 38 us -> 57.3 us
    all_gather x2 -> x0, blocking collectives: 55.3 us -> none  [gather_early(): lax.all_gather(piece, 'fs', axis=0, tiled=True, axis_index_groups=close)]
    ppermute x0 -> x3, waiting for transfers between devices: none -> 27.7 us  [the longest x1 16.8 us: gather_early(): beyond.append([near[k], lax.ppermute(far[k][1], 'fs', neighbour)])]
    ppermute x0 -> x3, starting transfers between devices: none -> 10.2 us  [the longest x2 8.3 us: gather_early(): near.append(lax.ppermute(own[k], 'fs', neighbour))]
    all_gather x1, blocking collectives: 75.1 us -> 80.2 us  [gather_early(): lax.all_gather(part, 'fs', axis=0, tiled=True, axis_index_groups=strided)]
    ppermute x4, starting transfers between devices: 27.4 us -> 32.4 us  [with_partner(): lax.ppermute(x, 'tp', [(k, k + 1 - 2 * (k % CORES)) for k in range(member...]
    ppermute x2 -> x3, starting transfers between devices: 6.02 us -> 9.52 us  [parts_of_all_groups(): behind.append(lax.ppermute(behind[-1], 'grp', up))]
  transfers between devices with their start and end apart: 8 -> 12, of which waited for: 5 -> 7; matrix products, arithmetic and copies ran while one was open for 1% -> 1% of each run, Pallas kernels for 2% -> 2%
where the time goes in v3:
time: 238 us
  blocking collectives  115 us (48%)
  starting transfers between devices  57.3 us (24%)
  waiting for transfers between devices  35.7 us (15%)
  between operations  13.6 us (6%)
  Pallas kernels  10.3 us (4%)
  other arithmetic  3.69 us (2%)
    all_gather x1, blocking collectives, gather_early(): lax.all_gather(part, 'fs', axis=0, tiled=True, axis_index_groups=strided)  80.2 us
    ppermute x4, starting transfers between devices, with_partner(): lax.ppermute(x, 'tp', [(k, k + 1 - 2 * (k % CORES)) for k in range(member...  32.4 us
    all_to_all x2, blocking collectives, summed_over_peers(): lax.all_to_all(pair.astype(jnp.bfloat16), 'tp', 0, 0, tiled=True, axis_in...  24.6 us
    ppermute x1, waiting for transfers between devices, gather_early(): beyond.append([near[k], lax.ppermute(far[k][1], 'fs', neighbour)])  16.8 us
    ppermute x2, waiting for transfers between devices, gather_early(): near.append(lax.ppermute(own[k], 'fs', neighbour))  10.8 us
    all_to_all x1, blocking collectives, from_everyone(): lax.all_to_all(copies, 'tp', 0, 0, tiled=True, axis_index_groups=groups)  10.3 us
    ppermute x3, starting transfers between devices, parts_of_all_groups(): behind.append(lax.ppermute(behind[-1], 'grp', up))  9.52 us
    ppermute x2, starting transfers between devices, gather_early(): near.append(lax.ppermute(own[k], 'fs', neighbour))  8.3 us
  transfers between devices with their start and end apart: 12, of which 7 were waited for; matrix products, arithmetic and copies ran while one was open for 1% of the time, Pallas kernels for 2%

profile of v3, /device:TPU:33, one launch (start us, length us, event | category | flops | bytes accessed | tf_op | source)
XLA Modules:
  0.0 237.5 jit_solution(10479758984558603868)
XLA Ops:
  6.6 1.7 pad_maximum_fusion
  8.3 1.8 broadcast_in_dim.18
  10.1 5.1 %all-to-all-start = ((bf16[4,256,256]{2,1,0:T(8,128)(2,1)}), bf16[4,256,256]{2,1,0:T(8,128)(2,1)S(1)}, u32[]{:S(2)}, u32[]{:S(2)}) async-start(bf16[4,256,256]{2,1,0:T(8,128)(2,1)} %broadcast_in_dim.18), calls=%async_computation | async-start | bytes 1048576 | tf_op jit(solution)/shard_map/all_to_all | solution.py:28
  15.2 0.8 fusion.1
  16.0 80.2 %all_gather.6 = bf16[512,768]{1,0:T(8,128)(2,1)S(1)} all-gather(bf16[32,768]{1,0:T(8,128)(2,1)S(1)} %fusion.1), channel_id=1, replica_groups={{0,16,32,48,64,80,96,112,128,144,160,176,192,208,224,240},{8,24,40,56,7..., dimensions={0}, use_global_device_ids=true | all-gather | bytes 835584 | tf_op jit(solution)/shard_map/all_gather | solution.py:91
  96.2 0.1 fusion.2
  96.3 4.7 %collective-permute-start.1 = (bf16[512,384]{1,0:T(8,128)(2,1)S(1)}, bf16[512,384]{1,0:T(8,128)(2,1)S(1)}, u32[]{:S(2)}, u32[]{:S(2)}) collective-permute-start(bf16[512,384]{1,0:T(8,128)(2,1)S(1)} %get-tuple-element.18.refs_1_), channel_id=1, source_target_pairs={{0,8},{8,0},{16,24},{24,16},{32,40},{40,32},{48,56},{56,48},{64,72... | collective-permute-start | bytes 1179656 | tf_op jit(solution)/shard_map/ppermute | solution.py:96
  101.0 4.1 %collective-permute-start.3 = (bf16[512,384]{1,0:T(8,128)(2,1)S(1)}, bf16[512,384]{1,0:T(8,128)(2,1)S(1)}, u32[]{:S(2)}, u32[]{:S(2)}) collective-permute-start(bf16[512,384]{1,0:T(8,128)(2,1)S(1)} %get-tuple-element.17.refs_5_), channel_id=1, source_target_pairs={{0,256},{256,0},{1,257},{257,1},{2,258},{258,2},{3,259},{259,3},{4... | collective-permute-start | bytes 1179656 | tf_op jit(solution)/shard_map/ppermute | solution.py:76
  105.1 9.6 %collective-permute-start.6 = (bf16[4,256,256]{2,1,0:T(8,128)(2,1)S(1)}, bf16[4,256,256]{2,1,0:T(8,128)(2,1)S(1)}, u32[]{:S(2)}, u32[]{:S(2)}) collective-permute-start(bf16[4,256,256]{2,1,0:T(8,128)(2,1)S(1)} %all-to-all-done.refs_9_), channel_id=1, source_target_pairs={{0,1},{1,0},{2,3},{3,2},{4,5},{5,4},{6,7},{7,6},{8,9},{9,8},{10,11... | collective-permute-start | bytes 1572872 | tf_op jit(solution)/shard_map/ppermute | solution.py:22
  114.7 2.0 collective-permute-start
  116.8 3.6 %collective-permute-start.4 = (bf16[512,384]{1,0:T(8,128)(2,1)S(1)}, bf16[512,384]{1,0:T(8,128)(2,1)S(1)}, u32[]{:S(2)}, u32[]{:S(2)}) collective-permute-start(bf16[512,384]{1,0:T(8,128)(2,1)S(1)} %get-tuple-element.17.refs_5_), channel_id=1, source_target_pairs={{0,8},{8,0},{16,24},{24,16},{32,40},{40,32},{48,56},{56,48},{64,72... | collective-permute-start | bytes 1179656 | tf_op jit(solution)/shard_map/ppermute | solution.py:96
  120.4 3.4 %collective-permute-start.2 = (bf16[512,384]{1,0:T(8,128)(2,1)S(1)}, bf16[512,384]{1,0:T(8,128)(2,1)}, u32[]{:S(2)}, u32[]{:S(2)}) collective-permute-start(bf16[512,384]{1,0:T(8,128)(2,1)S(1)} %collective-permute-done.1.refs_3_), channel_id=1, source_target_pairs={{0,256},{256,0},{1,257},{257,1},{2,258},{258,2},{3,259},{259,3},{4... | collective-permute-start | bytes 1179656 | tf_op jit(solution)/shard_map/ppermute | solution.py:76
  123.8 2.0 collective-permute-start.5
  125.8 0.1 pad_add_fusion.refs_0_
  125.8 1.6 collective-permute-done.refs_2_
  127.4 10.8 %collective-permute-done.4.refs_7_ = bf16[512,384]{1,0:T(8,128)(2,1)S(1)} collective-permute-done((bf16[512,384]{1,0:T(8,128)(2,1)S(1)}, bf16[512,384]{1,0:T(8,128)(2,1)S(1)}, u32[]{:S(2)}, u32[]{:S(2)}) %collective-permute-start.4) | collective-permute-done | bytes 393248 | tf_op jit(solution)/shard_map/ppermute | solution.py:96
  138.2 16.8 %collective-permute-done.5.refs_8_ = bf16[512,384]{1,0:T(8,128)(2,1)} collective-permute-done((bf16[512,384]{1,0:T(8,128)(2,1)S(1)}, bf16[512,384]{1,0:T(8,128)(2,1)}, u32[]{:S(2)}, u32[]{:S(2)}) %collective-permute-start.5) | collective-permute-done | bytes 393248 | tf_op jit(solution)/shard_map/ppermute | solution.py:101
  155.1 4.9 %recurrent.1 = (bf16[4,256,256]{2,1,0:T(8,128)(2,1)S(1)}, bf16[4,256,256]{2,1,0:T(8,128)(2,1)S(1)}) custom-call(s32[3]{0:T(128)S(1)} %pad_add_fusion.refs_0_, bf16[512,384]{1,0:T(8,128)(2,1)S(1)} %get-tuple-element.18.refs_1_, bf16[512,384]{1,0:T(8,128)(2,1)S(1)} %collective-permute-done.refs_2_, bf16[512,384]{1,0:T(8,128)(2,1)S(1)} %collective-permute-done.1.refs_3_, ...), custom_call_target="tpu_custom_call" | custom-call | flops 805306368 | bytes 5242880 | tf_op jit(solution)/shard_map/recurrent/pallas_call | solution.py:206
  160.0 4.7 %collective-permute-start.7 = (bf16[4,256,256]{2,1,0:T(8,128)(2,1)S(1)}, bf16[4,256,256]{2,1,0:T(8,128)(2,1)S(1)}, u32[]{:S(2)}, u32[]{:S(2)}) collective-permute-start(bf16[4,256,256]{2,1,0:T(8,128)(2,1)S(1)} %get-tuple-element.13), channel_id=1, source_target_pairs={{0,1},{1,0},{2,3},{3,2},{4,5},{5,4},{6,7},{7,6},{8,9},{9,8},{10,11... | collective-permute-start | bytes 1572872 | tf_op jit(solution)/shard_map/ppermute | solution.py:22
  164.7 1.5 collective-permute-done.7
  166.2 0.1 add_convert_fusion.1
  166.3 12.4 %all_to_all.20 = bf16[4,256,256]{2,1,0:T(8,128)(2,1)S(1)} all-to-all(bf16[4,256,256]{2,1,0:T(8,128)(2,1)S(1)} %add_convert_fusion.1), channel_id=1, replica_groups={{0,2,4,6},{1,3,5,7},{8,10,12,14},{9,11,13,15},{16,18,20,22},{17,19,21,2..., dimensions={0} | all-to-all | bytes 1048576 | tf_op jit(solution)/shard_map/all_to_all | solution.py:34
  178.9 10.3 %all_to_all.21.mine = bf16[4,256,256]{2,1,0:T(8,128)(2,1)S(1)} all-to-all(bf16[4,256,256]{2,1,0:T(8,128)(2,1)S(1)} %broadcast_in_dim.22), channel_id=1, replica_groups={{0,2,4,6},{1,3,5,7},{8,10,12,14},{9,11,13,15},{16,18,20,22},{17,19,21,2..., dimensions={0} | all-to-all | bytes 1048576 | tf_op jit(solution)/shard_map/all_to_all | solution.py:28
  189.1 4.5 %collective-permute-start.8 = (bf16[4,256,256]{2,1,0:T(8,128)(2,1)S(1)}, bf16[4,256,256]{2,1,0:T(8,128)(2,1)S(1)}, u32[]{:S(2)}, u32[]{:S(2)}) collective-permute-start(bf16[4,256,256]{2,1,0:T(8,128)(2,1)S(1)} %all_to_all.21.mine), channel_id=1, source_target_pairs={{0,1},{1,0},{2,3},{3,2},{4,5},{5,4},{6,7},{7,6},{8,9},{9,8},{10,11... | collective-permute-start | bytes 1572872 | tf_op jit(solution)/shard_map/ppermute | solution.py:22
  193.7 1.5 collective-permute-done.8.other
  195.2 1.9 all-gather.2.cloned.1.call-done.weights
  197.1 5.4 %feed_forward.1 = (bf16[4,256,256]{2,1,0:T(8,128)(2,1)S(1)}, bf16[4,256,256]{2,1,0:T(8,128)(2,1)S(1)}) custom-call(s32[1]{0:T(128)} %bitcast.2.core_ref, bf16[4,256,256]{2,1,0:T(8,128)(2,1)S(1)} %all_to_all.21.mine, bf16[4,256,256]{2,1,0:T(8,128)(2,1)S(1)} %collective-permute-done.8.other, f32[1,2048]{1,0:T(1,128)S(1)} %bitcast.9, ...), custom_call_target="tpu_custom_call" | custom-call | flops 2147483648 | bytes 10485760 | tf_op jit(solution)/shard_map/feed_forward/pallas_call | solution.py:281
  202.5 13.5 %collective-permute-start.9 = (bf16[4,256,256]{2,1,0:T(8,128)(2,1)S(1)}, bf16[4,256,256]{2,1,0:T(8,128)(2,1)S(1)}, u32[]{:S(2)}, u32[]{:S(2)}) collective-permute-start(bf16[4,256,256]{2,1,0:T(8,128)(2,1)S(1)} %get-tuple-element.16), channel_id=1, source_target_pairs={{0,1},{1,0},{2,3},{3,2},{4,5},{5,4},{6,7},{7,6},{8,9},{9,8},{10,11... | collective-permute-start | bytes 1572872 | tf_op jit(solution)/shard_map/ppermute | solution.py:22
  216.0 1.5 collective-permute-done.9
  217.5 0.1 add_convert_fusion
  217.6 12.3 %all_to_all.22 = bf16[4,256,256]{2,1,0:T(8,128)(2,1)S(1)} all-to-all(bf16[4,256,256]{2,1,0:T(8,128)(2,1)S(1)} %add_convert_fusion), channel_id=1, replica_groups={{0,2,4,6},{1,3,5,7},{8,10,12,14},{9,11,13,15},{16,18,20,22},{17,19,21,2..., dimensions={0} | all-to-all | bytes 1048576 | tf_op jit(solution)/shard_map/all_to_all | solution.py:34
  230.0 0.7 add_convert_fusion.2
  (15 shorter events, 0.3 us)
Async XLA Ops:
  6.5 172.2 %copy-start.1 = (bf16[256,256]{1,0:T(8,128)(2,1)S(1)}, bf16[256,256]{1,0:T(8,128)(2,1)}, u32[]{:S(2)}) copy-start(bf16[256,256]{1,0:T(8,128)(2,1)} %param.13) | copy-start | bytes 393220
  6.5 190.5 %copy-start = (f32[2048]{0:T(1024)S(1)}, f32[2048]{0:T(1024)}, u32[]{:S(2)}) copy-start(f32[2048]{0:T(1024)} %param.15) | copy-start | bytes 24580
  6.6 190.5 %all-gather.2.cloned.1.call-start = ((), (), s32[]{:S(2)}) async-start(), calls=%async_computation.4 | async-start | bytes 8650752 | tf_op jit(solution)/shard_map/all_gather | solution.py:326
  10.1 95.0 %all-to-all-start = ((bf16[4,256,256]{2,1,0:T(8,128)(2,1)}), bf16[4,256,256]{2,1,0:T(8,128)(2,1)S(1)}, u32[]{:S(2)}, u32[]{:S(2)}) async-start(bf16[4,256,256]{2,1,0:T(8,128)(2,1)} %broadcast_in_dim.18), calls=%async_computation | async-start | bytes 1048576 | tf_op jit(solution)/shard_map/all_to_all | solution.py:28
  96.3 24.1 %collective-permute-start.1 = (bf16[512,384]{1,0:T(8,128)(2,1)S(1)}, bf16[512,384]{1,0:T(8,128)(2,1)S(1)}, u32[]{:S(2)}, u32[]{:S(2)}) collective-permute-start(bf16[512,384]{1,0:T(8,128)(2,1)S(1)} %get-tuple-element.18.refs_1_), channel_id=1, source_target_pairs={{0,8},{8,0},{16,24},{24,16},{32,40},{40,32},{48,56},{56,48},{64,72... | collective-permute-start | bytes 1179656 | tf_op jit(solution)/shard_map/ppermute | solution.py:96
  101.0 22.8 %collective-permute-start.3 = (bf16[512,384]{1,0:T(8,128)(2,1)S(1)}, bf16[512,384]{1,0:T(8,128)(2,1)S(1)}, u32[]{:S(2)}, u32[]{:S(2)}) collective-permute-start(bf16[512,384]{1,0:T(8,128)(2,1)S(1)} %get-tuple-element.17.refs_5_), channel_id=1, source_target_pairs={{0,256},{256,0},{1,257},{257,1},{2,258},{258,2},{3,259},{259,3},{4... | collective-permute-start | bytes 1179656 | tf_op jit(solution)/shard_map/ppermute | solution.py:76
  105.1 50.0 %collective-permute-start.6 = (bf16[4,256,256]{2,1,0:T(8,128)(2,1)S(1)}, bf16[4,256,256]{2,1,0:T(8,128)(2,1)S(1)}, u32[]{:S(2)}, u32[]{:S(2)}) collective-permute-start(bf16[4,256,256]{2,1,0:T(8,128)(2,1)S(1)} %all-to-all-done.refs_9_), channel_id=1, source_target_pairs={{0,1},{1,0},{2,3},{3,2},{4,5},{5,4},{6,7},{7,6},{8,9},{9,8},{10,11... | collective-permute-start | bytes 1572872 | tf_op jit(solution)/shard_map/ppermute | solution.py:22
  114.7 12.7 %collective-permute-start = (bf16[512,384]{1,0:T(8,128)(2,1)S(1)}, bf16[512,384]{1,0:T(8,128)(2,1)S(1)}, u32[]{:S(2)}, u32[]{:S(2)}) collective-permute-start(bf16[512,384]{1,0:T(8,128)(2,1)S(1)} %get-tuple-element.18.refs_1_), channel_id=1, source_target_pairs={{0,256},{256,0},{1,257},{257,1},{2,258},{258,2},{3,259},{259,3},{4... | collective-permute-start | bytes 1179656 | tf_op jit(solution)/shard_map/ppermute | solution.py:76
  116.8 21.4 %collective-permute-start.4 = (bf16[512,384]{1,0:T(8,128)(2,1)S(1)}, bf16[512,384]{1,0:T(8,128)(2,1)S(1)}, u32[]{:S(2)}, u32[]{:S(2)}) collective-permute-start(bf16[512,384]{1,0:T(8,128)(2,1)S(1)} %get-tuple-element.17.refs_5_), channel_id=1, source_target_pairs={{0,8},{8,0},{16,24},{24,16},{32,40},{40,32},{48,56},{56,48},{64,72... | collective-permute-start | bytes 1179656 | tf_op jit(solution)/shard_map/ppermute | solution.py:96
  120.4 17.8 %collective-permute-start.2 = (bf16[512,384]{1,0:T(8,128)(2,1)S(1)}, bf16[512,384]{1,0:T(8,128)(2,1)}, u32[]{:S(2)}, u32[]{:S(2)}) collective-permute-start(bf16[512,384]{1,0:T(8,128)(2,1)S(1)} %collective-permute-done.1.refs_3_), channel_id=1, source_target_pairs={{0,256},{256,0},{1,257},{257,1},{2,258},{258,2},{3,259},{259,3},{4... | collective-permute-start | bytes 1179656 | tf_op jit(solution)/shard_map/ppermute | solution.py:76
  123.8 31.3 %collective-permute-start.5 = (bf16[512,384]{1,0:T(8,128)(2,1)S(1)}, bf16[512,384]{1,0:T(8,128)(2,1)}, u32[]{:S(2)}, u32[]{:S(2)}) collective-permute-start(bf16[512,384]{1,0:T(8,128)(2,1)S(1)} %collective-permute-done.3.refs_6_), channel_id=1, source_target_pairs={{0,8},{8,0},{16,24},{24,16},{32,40},{40,32},{48,56},{56,48},{64,72... | collective-permute-start | bytes 1179656 | tf_op jit(solution)/shard_map/ppermute | solution.py:101
  160.0 6.2 %collective-permute-start.7 = (bf16[4,256,256]{2,1,0:T(8,128)(2,1)S(1)}, bf16[4,256,256]{2,1,0:T(8,128)(2,1)S(1)}, u32[]{:S(2)}, u32[]{:S(2)}) collective-permute-start(bf16[4,256,256]{2,1,0:T(8,128)(2,1)S(1)} %get-tuple-element.13), channel_id=1, source_target_pairs={{0,1},{1,0},{2,3},{3,2},{4,5},{5,4},{6,7},{7,6},{8,9},{9,8},{10,11... | collective-permute-start | bytes 1572872 | tf_op jit(solution)/shard_map/ppermute | solution.py:22
  189.1 6.1 %collective-permute-start.8 = (bf16[4,256,256]{2,1,0:T(8,128)(2,1)S(1)}, bf16[4,256,256]{2,1,0:T(8,128)(2,1)S(1)}, u32[]{:S(2)}, u32[]{:S(2)}) collective-permute-start(bf16[4,256,256]{2,1,0:T(8,128)(2,1)S(1)} %all_to_all.21.mine), channel_id=1, source_target_pairs={{0,1},{1,0},{2,3},{3,2},{4,5},{5,4},{6,7},{7,6},{8,9},{9,8},{10,11... | collective-permute-start | bytes 1572872 | tf_op jit(solution)/shard_map/ppermute | solution.py:22
  202.5 15.0 %collective-permute-start.9 = (bf16[4,256,256]{2,1,0:T(8,128)(2,1)S(1)}, bf16[4,256,256]{2,1,0:T(8,128)(2,1)S(1)}, u32[]{:S(2)}, u32[]{:S(2)}) collective-permute-start(bf16[4,256,256]{2,1,0:T(8,128)(2,1)S(1)} %get-tuple-element.16), channel_id=1, source_target_pairs={{0,1},{1,0},{2,3},{3,2},{4,5},{5,4},{6,7},{7,6},{8,9},{9,8},{10,11... | collective-permute-start | bytes 1572872 | tf_op jit(solution)/shard_map/ppermute | solution.py:22
Sparse Core Ops, SparseCore 0:
  9.4 187.5 all-gather.1

commit v4 on v3

--- a/solution.py
+++ b/solution.py
@@ -87,20 +87,15 @@
     runs = ring // RUN
     part = lax.dynamic_slice_in_dim(shard, me * (rows // groups), rows // groups, 0)
     strided = [[k + RUN * j for j in range(runs)] for k in range(RUN)]
-    neighbour = [(k, k + 1 - 2 * (k % RUN)) for k in range(ring)]
+    turns = [[(k, (k + way) % ring) for k in range(ring)] for way in (1, -1)]
     level = lax.all_gather(part, "fs", axis=0, tiled=True, axis_index_groups=strided)
     wide = cols // PIECES
     own = [level[:, k * wide : (k + 1) * wide] for k in range(PIECES)]
     near = []
     for k in range(PIECES):
-        near.append(lax.ppermute(own[k], "fs", neighbour))
+        near.append(lax.ppermute(own[k], "fs", turns[k % 2]))
     far = [parts_of_all_groups(own[k]) for k in range(PIECES)]
-    beyond = []
-    for k in range(PIECES):
-        if groups == 2 and k == PIECES - 1:
-            beyond.append([near[k], lax.ppermute(far[k][1], "fs", neighbour)])
-        else:
-            beyond.append(parts_of_all_groups(near[k]))
+    beyond = [parts_of_all_groups(near[k]) for k in range(PIECES)]
     return [far[k] + beyond[k] for k in range(PIECES)], waiting
 
 

time: 238 us -> 227 us (0.954)
  starting transfers between devices: 57.3 us -> 50.3 us
  waiting for transfers between devices: 35.7 us -> 32 us
    ppermute x3 -> x2, waiting for transfers between devices: 27.7 us -> 0.01 us  [gather_early(): near.append(lax.ppermute(own[k], 'fs', turns[k % 2]))]
    ppermute x3 -> x4, waiting for transfers between devices: 1.58 us -> 27.4 us  [parts_of_all_groups(): behind.append(lax.ppermute(behind[-1], 'grp', up))]
    ppermute x4, starting transfers between devices: 32.4 us -> 25.2 us  [with_partner(): lax.ppermute(x, 'tp', [(k, k + 1 - 2 * (k % CORES)) for k in range(member...]
    ppermute x3 -> x4, starting transfers between devices: 9.52 us -> 12.9 us  [parts_of_all_groups(): behind.append(lax.ppermute(behind[-1], 'grp', up))]
    ppermute x3 -> x2, starting transfers between devices: 10.2 us -> 7.12 us  [gather_early(): near.append(lax.ppermute(own[k], 'fs', turns[k % 2]))]
where the time goes in v4:
time: 227 us; the launch traced here: 226 us
  blocking collectives  114 us (50%)
  starting transfers between devices  50.3 us (22%)
  waiting for transfers between devices  32 us (14%)
  between operations  13.6 us (6%)
  Pallas kernels  10.3 us (5%)
  other arithmetic  3.69 us (2%)
    all_gather x1, blocking collectives, gather_early(): lax.all_gather(part, 'fs', axis=0, tiled=True, axis_index_groups=strided)  80.2 us
    ppermute x4, waiting for transfers between devices, parts_of_all_groups(): behind.append(lax.ppermute(behind[-1], 'grp', up))  27.4 us
    ppermute x4, starting transfers between devices, with_partner(): lax.ppermute(x, 'tp', [(k, k + 1 - 2 * (k % CORES)) for k in range(member...  25.2 us
    all_to_all x2, blocking collectives, summed_over_peers(): lax.all_to_all(pair.astype(jnp.bfloat16), 'tp', 0, 0, tiled=True, axis_in...  23.9 us
    ppermute x4, starting transfers between devices, parts_of_all_groups(): behind.append(lax.ppermute(behind[-1], 'grp', up))  12.9 us
    all_to_all x1, blocking collectives, from_everyone(): lax.all_to_all(copies, 'tp', 0, 0, tiled=True, axis_index_groups=groups)  10.2 us
    ppermute x2, starting transfers between devices, gather_early(): near.append(lax.ppermute(own[k], 'fs', turns[k % 2]))  7.12 us
    pallas_call x1, Pallas kernels, feed_forward(): pl.pallas_call(feed_forward_body, out_shape=[jax.ShapeDtypeStruct(tiles[0...  5.39 us
  transfers between devices with their start and end apart: 12, of which 7 were waited for; matrix products, arithmetic and copies ran while one was open for 1% of the time, Pallas kernels for 2%

profile of v4, /device:TPU:33, one launch (start us, length us, event | category | flops | bytes accessed | tf_op | source)
XLA Modules:
  0.0 226.0 jit_solution(7275847433909644554)
XLA Ops:
  6.6 1.7 pad_maximum_fusion
  8.3 1.8 broadcast_in_dim.18
  10.1 5.1 %all-to-all-start = ((bf16[4,256,256]{2,1,0:T(8,128)(2,1)}), bf16[4,256,256]{2,1,0:T(8,128)(2,1)S(1)}, u32[]{:S(2)}, u32[]{:S(2)}) async-start(bf16[4,256,256]{2,1,0:T(8,128)(2,1)} %broadcast_in_dim.18), calls=%async_computation | async-start | bytes 1048576 | tf_op jit(solution)/shard_map/all_to_all | solution.py:28
  15.2 0.8 fusion.1
  16.0 80.2 %all_gather.6 = bf16[512,768]{1,0:T(8,128)(2,1)S(1)} all-gather(bf16[32,768]{1,0:T(8,128)(2,1)S(1)} %fusion.1), channel_id=1, replica_groups={{0,16,32,48,64,80,96,112,128,144,160,176,192,208,224,240},{8,24,40,56,7..., dimensions={0}, use_global_device_ids=true | all-gather | bytes 835584 | tf_op jit(solution)/shard_map/all_gather | solution.py:91
  96.2 0.1 fusion.2
  96.3 4.7 %collective-permute-start.1 = (bf16[512,384]{1,0:T(8,128)(2,1)S(1)}, bf16[512,384]{1,0:T(8,128)(2,1)S(1)}, u32[]{:S(2)}, u32[]{:S(2)}) collective-permute-start(bf16[512,384]{1,0:T(8,128)(2,1)S(1)} %get-tuple-element.18.refs_1_), channel_id=1, source_target_pairs={{0,8},{8,16},{16,24},{24,32},{32,40},{40,48},{48,56},{56,64},{64,7... | collective-permute-start | bytes 1179656 | tf_op jit(solution)/shard_map/ppermute | solution.py:96
  101.0 2.4 %collective-permute-start.4 = (bf16[512,384]{1,0:T(8,128)(2,1)S(1)}, bf16[512,384]{1,0:T(8,128)(2,1)S(1)}, u32[]{:S(2)}, u32[]{:S(2)}) collective-permute-start(bf16[512,384]{1,0:T(8,128)(2,1)S(1)} %get-tuple-element.17.refs_5_), channel_id=1, source_target_pairs={{0,248},{8,0},{16,8},{24,16},{32,24},{40,32},{48,40},{56,48},{64,5... | collective-permute-start | bytes 1179656 | tf_op jit(solution)/shard_map/ppermute | solution.py:96
  103.4 10.6 %collective-permute-start.6 = (bf16[4,256,256]{2,1,0:T(8,128)(2,1)S(1)}, bf16[4,256,256]{2,1,0:T(8,128)(2,1)S(1)}, u32[]{:S(2)}, u32[]{:S(2)}) collective-permute-start(bf16[4,256,256]{2,1,0:T(8,128)(2,1)S(1)} %all-to-all-done.refs_9_), channel_id=1, source_target_pairs={{0,1},{1,0},{2,3},{3,2},{4,5},{5,4},{6,7},{7,6},{8,9},{9,8},{10,11... | collective-permute-start | bytes 1572872 | tf_op jit(solution)/shard_map/ppermute | solution.py:22
  114.1 5.6 %collective-permute-start = (bf16[512,384]{1,0:T(8,128)(2,1)S(1)}, bf16[512,384]{1,0:T(8,128)(2,1)S(1)}, u32[]{:S(2)}, u32[]{:S(2)}) collective-permute-start(bf16[512,384]{1,0:T(8,128)(2,1)S(1)} %get-tuple-element.18.refs_1_), channel_id=1, source_target_pairs={{0,256},{256,0},{1,257},{257,1},{2,258},{258,2},{3,259},{259,3},{4... | collective-permute-start | bytes 1179656 | tf_op jit(solution)/shard_map/ppermute | solution.py:76
  119.6 2.0 collective-permute-start.3
  121.6 3.4 %collective-permute-start.2 = (bf16[512,384]{1,0:T(8,128)(2,1)S(1)}, bf16[512,384]{1,0:T(8,128)(2,1)}, u32[]{:S(2)}, u32[]{:S(2)}) collective-permute-start(bf16[512,384]{1,0:T(8,128)(2,1)S(1)} %collective-permute-done.1.refs_3_), channel_id=1, source_target_pairs={{0,256},{256,0},{1,257},{257,1},{2,258},{258,2},{3,259},{259,3},{4... | collective-permute-start | bytes 1179656 | tf_op jit(solution)/shard_map/ppermute | solution.py:76
  125.0 2.0 collective-permute-start.5
  127.0 0.1 pad_add_fusion.refs_0_
  127.1 2.1 collective-permute-done.refs_2_
  129.2 8.4 %collective-permute-done.3.refs_6_ = bf16[512,384]{1,0:T(8,128)(2,1)S(1)} collective-permute-done((bf16[512,384]{1,0:T(8,128)(2,1)S(1)}, bf16[512,384]{1,0:T(8,128)(2,1)S(1)}, u32[]{:S(2)}, u32[]{:S(2)}) %collective-permute-start.3) | collective-permute-done | bytes 393248 | tf_op jit(solution)/shard_map/ppermute | solution.py:76
  137.6 8.4 %collective-permute-done.2.refs_4_ = bf16[512,384]{1,0:T(8,128)(2,1)} collective-permute-done((bf16[512,384]{1,0:T(8,128)(2,1)S(1)}, bf16[512,384]{1,0:T(8,128)(2,1)}, u32[]{:S(2)}, u32[]{:S(2)}) %collective-permute-start.2) | collective-permute-done | bytes 393248 | tf_op jit(solution)/shard_map/ppermute | solution.py:76
  146.0 8.4 %collective-permute-done.5.refs_8_ = bf16[512,384]{1,0:T(8,128)(2,1)} collective-permute-done((bf16[512,384]{1,0:T(8,128)(2,1)S(1)}, bf16[512,384]{1,0:T(8,128)(2,1)}, u32[]{:S(2)}, u32[]{:S(2)}) %collective-permute-start.5) | collective-permute-done | bytes 393248 | tf_op jit(solution)/shard_map/ppermute | solution.py:76
  154.5 4.9 %recurrent.1 = (bf16[4,256,256]{2,1,0:T(8,128)(2,1)S(1)}, bf16[4,256,256]{2,1,0:T(8,128)(2,1)S(1)}) custom-call(s32[3]{0:T(128)S(1)} %pad_add_fusion.refs_0_, bf16[512,384]{1,0:T(8,128)(2,1)S(1)} %get-tuple-element.18.refs_1_, bf16[512,384]{1,0:T(8,128)(2,1)S(1)} %collective-permute-done.refs_2_, bf16[512,384]{1,0:T(8,128)(2,1)S(1)} %collective-permute-done.1.refs_3_, ...), custom_call_target="tpu_custom_call" | custom-call | flops 805306368 | bytes 5242880 | tf_op jit(solution)/shard_map/recurrent/pallas_call | solution.py:201
  159.3 2.5 %collective-permute-start.7 = (bf16[4,256,256]{2,1,0:T(8,128)(2,1)S(1)}, bf16[4,256,256]{2,1,0:T(8,128)(2,1)S(1)}, u32[]{:S(2)}, u32[]{:S(2)}) collective-permute-start(bf16[4,256,256]{2,1,0:T(8,128)(2,1)S(1)} %get-tuple-element.13), channel_id=1, source_target_pairs={{0,1},{1,0},{2,3},{3,2},{4,5},{5,4},{6,7},{7,6},{8,9},{9,8},{10,11... | collective-permute-start | bytes 1572872 | tf_op jit(solution)/shard_map/ppermute | solution.py:22
  161.9 1.5 collective-permute-done.7
  163.4 0.1 add_convert_fusion.1
  163.5 11.6 %all_to_all.20 = bf16[4,256,256]{2,1,0:T(8,128)(2,1)S(1)} all-to-all(bf16[4,256,256]{2,1,0:T(8,128)(2,1)S(1)} %add_convert_fusion.1), channel_id=1, replica_groups={{0,2,4,6},{1,3,5,7},{8,10,12,14},{9,11,13,15},{16,18,20,22},{17,19,21,2..., dimensions={0} | all-to-all | bytes 1048576 | tf_op jit(solution)/shard_map/all_to_all | solution.py:34
  175.3 10.2 %all_to_all.21.mine = bf16[4,256,256]{2,1,0:T(8,128)(2,1)S(1)} all-to-all(bf16[4,256,256]{2,1,0:T(8,128)(2,1)S(1)} %broadcast_in_dim.22), channel_id=1, replica_groups={{0,2,4,6},{1,3,5,7},{8,10,12,14},{9,11,13,15},{16,18,20,22},{17,19,21,2..., dimensions={0} | all-to-all | bytes 1048576 | tf_op jit(solution)/shard_map/all_to_all | solution.py:28
  185.5 4.6 %collective-permute-start.8 = (bf16[4,256,256]{2,1,0:T(8,128)(2,1)S(1)}, bf16[4,256,256]{2,1,0:T(8,128)(2,1)S(1)}, u32[]{:S(2)}, u32[]{:S(2)}) collective-permute-start(bf16[4,256,256]{2,1,0:T(8,128)(2,1)S(1)} %all_to_all.21.mine), channel_id=1, source_target_pairs={{0,1},{1,0},{2,3},{3,2},{4,5},{5,4},{6,7},{7,6},{8,9},{9,8},{10,11... | collective-permute-start | bytes 1572872 | tf_op jit(solution)/shard_map/ppermute | solution.py:22
  190.1 1.5 collective-permute-done.8.other
  191.6 5.4 %feed_forward.1 = (bf16[4,256,256]{2,1,0:T(8,128)(2,1)S(1)}, bf16[4,256,256]{2,1,0:T(8,128)(2,1)S(1)}) custom-call(s32[1]{0:T(128)} %bitcast.2.core_ref, bf16[4,256,256]{2,1,0:T(8,128)(2,1)S(1)} %all_to_all.21.mine, bf16[4,256,256]{2,1,0:T(8,128)(2,1)S(1)} %collective-permute-done.8.other, f32[1,2048]{1,0:T(1,128)S(1)} %bitcast.9, ...), custom_call_target="tpu_custom_call" | custom-call | flops 2147483648 | bytes 10485760 | tf_op jit(solution)/shard_map/feed_forward/pallas_call | solution.py:276
  197.0 7.5 %collective-permute-start.9 = (bf16[4,256,256]{2,1,0:T(8,128)(2,1)S(1)}, bf16[4,256,256]{2,1,0:T(8,128)(2,1)S(1)}, u32[]{:S(2)}, u32[]{:S(2)}) collective-permute-start(bf16[4,256,256]{2,1,0:T(8,128)(2,1)S(1)} %get-tuple-element.16), channel_id=1, source_target_pairs={{0,1},{1,0},{2,3},{3,2},{4,5},{5,4},{6,7},{7,6},{8,9},{9,8},{10,11... | collective-permute-start | bytes 1572872 | tf_op jit(solution)/shard_map/ppermute | solution.py:22
  204.5 1.5 collective-permute-done.9
  206.0 0.1 add_convert_fusion
  206.1 12.3 %all_to_all.22 = bf16[4,256,256]{2,1,0:T(8,128)(2,1)S(1)} all-to-all(bf16[4,256,256]{2,1,0:T(8,128)(2,1)S(1)} %add_convert_fusion), channel_id=1, replica_groups={{0,2,4,6},{1,3,5,7},{8,10,12,14},{9,11,13,15},{16,18,20,22},{17,19,21,2..., dimensions={0} | all-to-all | bytes 1048576 | tf_op jit(solution)/shard_map/all_to_all | solution.py:34
  218.5 0.7 add_convert_fusion.2
  (15 shorter events, 0.3 us)
Async XLA Ops:
  6.5 168.7 %copy-start.1 = (bf16[256,256]{1,0:T(8,128)(2,1)S(1)}, bf16[256,256]{1,0:T(8,128)(2,1)}, u32[]{:S(2)}) copy-start(bf16[256,256]{1,0:T(8,128)(2,1)} %param.13) | copy-start | bytes 393220
  6.5 185.1 %copy-start = (f32[2048]{0:T(1024)S(1)}, f32[2048]{0:T(1024)}, u32[]{:S(2)}) copy-start(f32[2048]{0:T(1024)} %param.15) | copy-start | bytes 24580
  6.6 185.1 %all-gather.2.cloned.1.call-start = ((), (), s32[]{:S(2)}) async-start(), calls=%async_computation.4 | async-start | bytes 8650752 | tf_op jit(solution)/shard_map/all_gather | solution.py:321
  10.1 93.3 %all-to-all-start = ((bf16[4,256,256]{2,1,0:T(8,128)(2,1)}), bf16[4,256,256]{2,1,0:T(8,128)(2,1)S(1)}, u32[]{:S(2)}, u32[]{:S(2)}) async-start(bf16[4,256,256]{2,1,0:T(8,128)(2,1)} %broadcast_in_dim.18), calls=%async_computation | async-start | bytes 1048576 | tf_op jit(solution)/shard_map/all_to_all | solution.py:28
  96.3 25.3 %collective-permute-start.1 = (bf16[512,384]{1,0:T(8,128)(2,1)S(1)}, bf16[512,384]{1,0:T(8,128)(2,1)S(1)}, u32[]{:S(2)}, u32[]{:S(2)}) collective-permute-start(bf16[512,384]{1,0:T(8,128)(2,1)S(1)} %get-tuple-element.18.refs_1_), channel_id=1, source_target_pairs={{0,8},{8,16},{16,24},{24,32},{32,40},{40,48},{48,56},{56,64},{64,7... | collective-permute-start | bytes 1179656 | tf_op jit(solution)/shard_map/ppermute | solution.py:96
  101.0 24.0 %collective-permute-start.4 = (bf16[512,384]{1,0:T(8,128)(2,1)S(1)}, bf16[512,384]{1,0:T(8,128)(2,1)S(1)}, u32[]{:S(2)}, u32[]{:S(2)}) collective-permute-start(bf16[512,384]{1,0:T(8,128)(2,1)S(1)} %get-tuple-element.17.refs_5_), channel_id=1, source_target_pairs={{0,248},{8,0},{16,8},{24,16},{32,24},{40,32},{48,40},{56,48},{64,5... | collective-permute-start | bytes 1179656 | tf_op jit(solution)/shard_map/ppermute | solution.py:96
  103.4 51.1 %collective-permute-start.6 = (bf16[4,256,256]{2,1,0:T(8,128)(2,1)S(1)}, bf16[4,256,256]{2,1,0:T(8,128)(2,1)S(1)}, u32[]{:S(2)}, u32[]{:S(2)}) collective-permute-start(bf16[4,256,256]{2,1,0:T(8,128)(2,1)S(1)} %all-to-all-done.refs_9_), channel_id=1, source_target_pairs={{0,1},{1,0},{2,3},{3,2},{4,5},{5,4},{6,7},{7,6},{8,9},{9,8},{10,11... | collective-permute-start | bytes 1572872 | tf_op jit(solution)/shard_map/ppermute | solution.py:22
  114.1 15.1 %collective-permute-start = (bf16[512,384]{1,0:T(8,128)(2,1)S(1)}, bf16[512,384]{1,0:T(8,128)(2,1)S(1)}, u32[]{:S(2)}, u32[]{:S(2)}) collective-permute-start(bf16[512,384]{1,0:T(8,128)(2,1)S(1)} %get-tuple-element.18.refs_1_), channel_id=1, source_target_pairs={{0,256},{256,0},{1,257},{257,1},{2,258},{258,2},{3,259},{259,3},{4... | collective-permute-start | bytes 1179656 | tf_op jit(solution)/shard_map/ppermute | solution.py:76
  119.6 18.0 %collective-permute-start.3 = (bf16[512,384]{1,0:T(8,128)(2,1)S(1)}, bf16[512,384]{1,0:T(8,128)(2,1)S(1)}, u32[]{:S(2)}, u32[]{:S(2)}) collective-permute-start(bf16[512,384]{1,0:T(8,128)(2,1)S(1)} %get-tuple-element.17.refs_5_), channel_id=1, source_target_pairs={{0,256},{256,0},{1,257},{257,1},{2,258},{258,2},{3,259},{259,3},{4... | collective-permute-start | bytes 1179656 | tf_op jit(solution)/shard_map/ppermute | solution.py:76
  121.6 24.5 %collective-permute-start.2 = (bf16[512,384]{1,0:T(8,128)(2,1)S(1)}, bf16[512,384]{1,0:T(8,128)(2,1)}, u32[]{:S(2)}, u32[]{:S(2)}) collective-permute-start(bf16[512,384]{1,0:T(8,128)(2,1)S(1)} %collective-permute-done.1.refs_3_), channel_id=1, source_target_pairs={{0,256},{256,0},{1,257},{257,1},{2,258},{258,2},{3,259},{259,3},{4... | collective-permute-start | bytes 1179656 | tf_op jit(solution)/shard_map/ppermute | solution.py:76
  125.0 29.5 %collective-permute-start.5 = (bf16[512,384]{1,0:T(8,128)(2,1)S(1)}, bf16[512,384]{1,0:T(8,128)(2,1)}, u32[]{:S(2)}, u32[]{:S(2)}) collective-permute-start(bf16[512,384]{1,0:T(8,128)(2,1)S(1)} %collective-permute-done.4.refs_7_), channel_id=1, source_target_pairs={{0,256},{256,0},{1,257},{257,1},{2,258},{258,2},{3,259},{259,3},{4... | collective-permute-start | bytes 1179656 | tf_op jit(solution)/shard_map/ppermute | solution.py:76
  159.3 4.1 %collective-permute-start.7 = (bf16[4,256,256]{2,1,0:T(8,128)(2,1)S(1)}, bf16[4,256,256]{2,1,0:T(8,128)(2,1)S(1)}, u32[]{:S(2)}, u32[]{:S(2)}) collective-permute-start(bf16[4,256,256]{2,1,0:T(8,128)(2,1)S(1)} %get-tuple-element.13), channel_id=1, source_target_pairs={{0,1},{1,0},{2,3},{3,2},{4,5},{5,4},{6,7},{7,6},{8,9},{9,8},{10,11... | collective-permute-start | bytes 1572872 | tf_op jit(solution)/shard_map/ppermute | solution.py:22
  185.5 6.1 %collective-permute-start.8 = (bf16[4,256,256]{2,1,0:T(8,128)(2,1)S(1)}, bf16[4,256,256]{2,1,0:T(8,128)(2,1)S(1)}, u32[]{:S(2)}, u32[]{:S(2)}) collective-permute-start(bf16[4,256,256]{2,1,0:T(8,128)(2,1)S(1)} %all_to_all.21.mine), channel_id=1, source_target_pairs={{0,1},{1,0},{2,3},{3,2},{4,5},{5,4},{6,7},{7,6},{8,9},{9,8},{10,11... | collective-permute-start | bytes 1572872 | tf_op jit(solution)/shard_map/ppermute | solution.py:22
  197.0 9.0 %collective-permute-start.9 = (bf16[4,256,256]{2,1,0:T(8,128)(2,1)S(1)}, bf16[4,256,256]{2,1,0:T(8,128)(2,1)S(1)}, u32[]{:S(2)}, u32[]{:S(2)}) collective-permute-start(bf16[4,256,256]{2,1,0:T(8,128)(2,1)S(1)} %get-tuple-element.16), channel_id=1, source_target_pairs={{0,1},{1,0},{2,3},{3,2},{4,5},{5,4},{6,7},{7,6},{8,9},{9,8},{10,11... | collective-permute-start | bytes 1572872 | tf_op jit(solution)/shard_map/ppermute | solution.py:22
Sparse Core Ops, SparseCore 0:
  9.4 173.2 all-gather.1

commit v5 on v4

--- a/solution.py
+++ b/solution.py
@@ -86,7 +86,7 @@
     ring = lax.axis_size("fs")
     runs = ring // RUN
     part = lax.dynamic_slice_in_dim(shard, me * (rows // groups), rows // groups, 0)
-    strided = [[k + RUN * j for j in range(runs)] for k in range(RUN)]
+    strided = [[k + RUN * j for j in range(runs)][:: 1 - 2 * k] for k in range(RUN)]
     turns = [[(k, (k + way) % ring) for k in range(ring)] for way in (1, -1)]
     level = lax.all_gather(part, "fs", axis=0, tiled=True, axis_index_groups=strided)
     wide = cols // PIECES
@@ -121,9 +121,10 @@
     for behind in range(groups):
         place = lax.rem(me_ref[0] + groups - behind, groups) * each
         for side in range(RUN):
-            near = lax.rem(me_ref[2] + side, RUN) * groups * each
+            odd = lax.rem(me_ref[2] + side, RUN)
             for far in range(runs):
-                to = pl.multiple_of(far * RUN * groups * each + near + place, each)
+                at = (far + odd * (runs - 1 - 2 * far)) * RUN + odd
+                to = pl.multiple_of(at * groups * each + place, each)
                 for piece in range(pieces):
                     weights[pl.ds(to, each), piece * wide : (piece + 1) * wide] = parts[
                         (piece * RUN + side) * groups + behind

time: 227 us -> 226 us (level)
  no operation moved by 1% of the time
where the time goes in v5:
time: 226 us; the launch traced here: 225 us
  blocking collectives  115 us (51%)
  starting transfers between devices  48.3 us (21%)
  waiting for transfers between devices  32 us (14%)
  between operations  13.6 us (6%)
  Pallas kernels  10.4 us (5%)
  other arithmetic  3.69 us (2%)
    all_gather x1, blocking collectives, gather_early(): lax.all_gather(part, 'fs', axis=0, tiled=True, axis_index_groups=strided)  80.7 us
    ppermute x4, waiting for transfers between devices, parts_of_all_groups(): behind.append(lax.ppermute(behind[-1], 'grp', up))  27.4 us
    all_to_all x2, blocking collectives, summed_over_peers(): lax.all_to_all(pair.astype(jnp.bfloat16), 'tp', 0, 0, tiled=True, axis_in...  23.8 us
    ppermute x4, starting transfers between devices, with_partner(): lax.ppermute(x, 'tp', [(k, k + 1 - 2 * (k % CORES)) for k in range(member...  23.1 us
    ppermute x4, starting transfers between devices, parts_of_all_groups(): behind.append(lax.ppermute(behind[-1], 'grp', up))  12.7 us
    all_to_all x1, blocking collectives, from_everyone(): lax.all_to_all(copies, 'tp', 0, 0, tiled=True, axis_index_groups=groups)  10.3 us
    ppermute x2, starting transfers between devices, gather_early(): near.append(lax.ppermute(own[k], 'fs', turns[k % 2]))  7.4 us
    pallas_call x1, Pallas kernels, feed_forward(): pl.pallas_call(feed_forward_body, out_shape=[jax.ShapeDtypeStruct(tiles[0...  5.4 us
  transfers between devices with their start and end apart: 12, of which 7 were waited for; matrix products, arithmetic and copies ran while one was open for 1% of the time, Pallas kernels for 2%

profile of v5, /device:TPU:33, one launch (start us, length us, event | category | flops | bytes accessed | tf_op | source)
XLA Modules:
  0.0 224.6 jit_solution(4656819362339460627)
XLA Ops:
  6.6 1.7 pad_maximum_fusion
  8.3 1.8 broadcast_in_dim.18
  10.1 5.1 %all-to-all-start = ((bf16[4,256,256]{2,1,0:T(8,128)(2,1)}), bf16[4,256,256]{2,1,0:T(8,128)(2,1)S(1)}, u32[]{:S(2)}, u32[]{:S(2)}) async-start(bf16[4,256,256]{2,1,0:T(8,128)(2,1)} %broadcast_in_dim.18), calls=%async_computation | async-start | bytes 1048576 | tf_op jit(solution)/shard_map/all_to_all | solution.py:28
  15.2 0.8 fusion.1
  16.0 80.7 %all_gather.6 = bf16[512,768]{1,0:T(8,128)(2,1)S(1)} all-gather(bf16[32,768]{1,0:T(8,128)(2,1)S(1)} %fusion.1), channel_id=1, replica_groups={{0,16,32,48,64,80,96,112,128,144,160,176,192,208,224,240},{248,232,216,..., dimensions={0}, use_global_device_ids=true | all-gather | bytes 835584 | tf_op jit(solution)/shard_map/all_gather | solution.py:91
  96.6 0.1 fusion.2
  96.7 4.1 %collective-permute-start.1 = (bf16[512,384]{1,0:T(8,128)(2,1)S(1)}, bf16[512,384]{1,0:T(8,128)(2,1)S(1)}, u32[]{:S(2)}, u32[]{:S(2)}) collective-permute-start(bf16[512,384]{1,0:T(8,128)(2,1)S(1)} %get-tuple-element.18.refs_1_), channel_id=1, source_target_pairs={{0,8},{8,16},{16,24},{24,32},{32,40},{40,48},{48,56},{56,64},{64,7... | collective-permute-start | bytes 1179656 | tf_op jit(solution)/shard_map/ppermute | solution.py:96
  100.8 3.3 %collective-permute-start.4 = (bf16[512,384]{1,0:T(8,128)(2,1)S(1)}, bf16[512,384]{1,0:T(8,128)(2,1)S(1)}, u32[]{:S(2)}, u32[]{:S(2)}) collective-permute-start(bf16[512,384]{1,0:T(8,128)(2,1)S(1)} %get-tuple-element.17.refs_5_), channel_id=1, source_target_pairs={{0,248},{8,0},{16,8},{24,16},{32,24},{40,32},{48,40},{56,48},{64,5... | collective-permute-start | bytes 1179656 | tf_op jit(solution)/shard_map/ppermute | solution.py:96
  104.2 9.7 %collective-permute-start.6 = (bf16[4,256,256]{2,1,0:T(8,128)(2,1)S(1)}, bf16[4,256,256]{2,1,0:T(8,128)(2,1)S(1)}, u32[]{:S(2)}, u32[]{:S(2)}) collective-permute-start(bf16[4,256,256]{2,1,0:T(8,128)(2,1)S(1)} %all-to-all-done.refs_9_), channel_id=1, source_target_pairs={{0,1},{1,0},{2,3},{3,2},{4,5},{5,4},{6,7},{7,6},{8,9},{9,8},{10,11... | collective-permute-start | bytes 1572872 | tf_op jit(solution)/shard_map/ppermute | solution.py:22
  113.9 5.4 %collective-permute-start = (bf16[512,384]{1,0:T(8,128)(2,1)S(1)}, bf16[512,384]{1,0:T(8,128)(2,1)S(1)}, u32[]{:S(2)}, u32[]{:S(2)}) collective-permute-start(bf16[512,384]{1,0:T(8,128)(2,1)S(1)} %get-tuple-element.18.refs_1_), channel_id=1, source_target_pairs={{0,256},{256,0},{1,257},{257,1},{2,258},{258,2},{3,259},{259,3},{4... | collective-permute-start | bytes 1179656 | tf_op jit(solution)/shard_map/ppermute | solution.py:76
  119.3 2.0 collective-permute-start.3
  121.3 3.4 %collective-permute-start.2 = (bf16[512,384]{1,0:T(8,128)(2,1)S(1)}, bf16[512,384]{1,0:T(8,128)(2,1)}, u32[]{:S(2)}, u32[]{:S(2)}) collective-permute-start(bf16[512,384]{1,0:T(8,128)(2,1)S(1)} %collective-permute-done.1.refs_3_), channel_id=1, source_target_pairs={{0,256},{256,0},{1,257},{257,1},{2,258},{258,2},{3,259},{259,3},{4... | collective-permute-start | bytes 1179656 | tf_op jit(solution)/shard_map/ppermute | solution.py:76
  124.7 2.0 collective-permute-start.5
  126.6 0.1 pad_add_fusion.refs_0_
  126.7 2.1 collective-permute-done.refs_2_
  128.9 8.4 %collective-permute-done.3.refs_6_ = bf16[512,384]{1,0:T(8,128)(2,1)S(1)} collective-permute-done((bf16[512,384]{1,0:T(8,128)(2,1)S(1)}, bf16[512,384]{1,0:T(8,128)(2,1)S(1)}, u32[]{:S(2)}, u32[]{:S(2)}) %collective-permute-start.3) | collective-permute-done | bytes 393248 | tf_op jit(solution)/shard_map/ppermute | solution.py:76
  137.3 8.4 %collective-permute-done.2.refs_4_ = bf16[512,384]{1,0:T(8,128)(2,1)} collective-permute-done((bf16[512,384]{1,0:T(8,128)(2,1)S(1)}, bf16[512,384]{1,0:T(8,128)(2,1)}, u32[]{:S(2)}, u32[]{:S(2)}) %collective-permute-start.2) | collective-permute-done | bytes 393248 | tf_op jit(solution)/shard_map/ppermute | solution.py:76
  145.7 8.4 %collective-permute-done.5.refs_8_ = bf16[512,384]{1,0:T(8,128)(2,1)} collective-permute-done((bf16[512,384]{1,0:T(8,128)(2,1)S(1)}, bf16[512,384]{1,0:T(8,128)(2,1)}, u32[]{:S(2)}, u32[]{:S(2)}) %collective-permute-start.5) | collective-permute-done | bytes 393248 | tf_op jit(solution)/shard_map/ppermute | solution.py:76
  154.1 5.0 %recurrent.1 = (bf16[4,256,256]{2,1,0:T(8,128)(2,1)S(1)}, bf16[4,256,256]{2,1,0:T(8,128)(2,1)S(1)}) custom-call(s32[3]{0:T(128)S(1)} %pad_add_fusion.refs_0_, bf16[512,384]{1,0:T(8,128)(2,1)S(1)} %get-tuple-element.18.refs_1_, bf16[512,384]{1,0:T(8,128)(2,1)S(1)} %collective-permute-done.refs_2_, bf16[512,384]{1,0:T(8,128)(2,1)S(1)} %collective-permute-done.1.refs_3_, ...), custom_call_target="tpu_custom_call" | custom-call | flops 805306368 | bytes 5242880 | tf_op jit(solution)/shard_map/recurrent/pallas_call | solution.py:202
  159.1 2.5 %collective-permute-start.7 = (bf16[4,256,256]{2,1,0:T(8,128)(2,1)S(1)}, bf16[4,256,256]{2,1,0:T(8,128)(2,1)S(1)}, u32[]{:S(2)}, u32[]{:S(2)}) collective-permute-start(bf16[4,256,256]{2,1,0:T(8,128)(2,1)S(1)} %get-tuple-element.13), channel_id=1, source_target_pairs={{0,1},{1,0},{2,3},{3,2},{4,5},{5,4},{6,7},{7,6},{8,9},{9,8},{10,11... | collective-permute-start | bytes 1572872 | tf_op jit(solution)/shard_map/ppermute | solution.py:22
  161.7 1.5 collective-permute-done.7
  163.2 0.1 add_convert_fusion.1
  163.3 12.3 %all_to_all.20 = bf16[4,256,256]{2,1,0:T(8,128)(2,1)S(1)} all-to-all(bf16[4,256,256]{2,1,0:T(8,128)(2,1)S(1)} %add_convert_fusion.1), channel_id=1, replica_groups={{0,2,4,6},{1,3,5,7},{8,10,12,14},{9,11,13,15},{16,18,20,22},{17,19,21,2..., dimensions={0} | all-to-all | bytes 1048576 | tf_op jit(solution)/shard_map/all_to_all | solution.py:34
  175.8 10.3 %all_to_all.21.mine = bf16[4,256,256]{2,1,0:T(8,128)(2,1)S(1)} all-to-all(bf16[4,256,256]{2,1,0:T(8,128)(2,1)S(1)} %broadcast_in_dim.22), channel_id=1, replica_groups={{0,2,4,6},{1,3,5,7},{8,10,12,14},{9,11,13,15},{16,18,20,22},{17,19,21,2..., dimensions={0} | all-to-all | bytes 1048576 | tf_op jit(solution)/shard_map/all_to_all | solution.py:28
  186.0 4.5 %collective-permute-start.8 = (bf16[4,256,256]{2,1,0:T(8,128)(2,1)S(1)}, bf16[4,256,256]{2,1,0:T(8,128)(2,1)S(1)}, u32[]{:S(2)}, u32[]{:S(2)}) collective-permute-start(bf16[4,256,256]{2,1,0:T(8,128)(2,1)S(1)} %all_to_all.21.mine), channel_id=1, source_target_pairs={{0,1},{1,0},{2,3},{3,2},{4,5},{5,4},{6,7},{7,6},{8,9},{9,8},{10,11... | collective-permute-start | bytes 1572872 | tf_op jit(solution)/shard_map/ppermute | solution.py:22
  190.6 1.5 collective-permute-done.8.other
  192.1 5.4 %feed_forward.1 = (bf16[4,256,256]{2,1,0:T(8,128)(2,1)S(1)}, bf16[4,256,256]{2,1,0:T(8,128)(2,1)S(1)}) custom-call(s32[1]{0:T(128)} %bitcast.2.core_ref, bf16[4,256,256]{2,1,0:T(8,128)(2,1)S(1)} %all_to_all.21.mine, bf16[4,256,256]{2,1,0:T(8,128)(2,1)S(1)} %collective-permute-done.8.other, f32[1,2048]{1,0:T(1,128)S(1)} %bitcast.9, ...), custom_call_target="tpu_custom_call" | custom-call | flops 2147483648 | bytes 10485760 | tf_op jit(solution)/shard_map/feed_forward/pallas_call | solution.py:277
  197.5 6.3 %collective-permute-start.9 = (bf16[4,256,256]{2,1,0:T(8,128)(2,1)S(1)}, bf16[4,256,256]{2,1,0:T(8,128)(2,1)S(1)}, u32[]{:S(2)}, u32[]{:S(2)}) collective-permute-start(bf16[4,256,256]{2,1,0:T(8,128)(2,1)S(1)} %get-tuple-element.16), channel_id=1, source_target_pairs={{0,1},{1,0},{2,3},{3,2},{4,5},{5,4},{6,7},{7,6},{8,9},{9,8},{10,11... | collective-permute-start | bytes 1572872 | tf_op jit(solution)/shard_map/ppermute | solution.py:22
  203.8 1.5 collective-permute-done.9
  205.3 0.1 add_convert_fusion
  205.4 11.5 %all_to_all.22 = bf16[4,256,256]{2,1,0:T(8,128)(2,1)S(1)} all-to-all(bf16[4,256,256]{2,1,0:T(8,128)(2,1)S(1)} %add_convert_fusion), channel_id=1, replica_groups={{0,2,4,6},{1,3,5,7},{8,10,12,14},{9,11,13,15},{16,18,20,22},{17,19,21,2..., dimensions={0} | all-to-all | bytes 1048576 | tf_op jit(solution)/shard_map/all_to_all | solution.py:34
  217.0 0.7 add_convert_fusion.2
  (15 shorter events, 0.3 us)
Async XLA Ops:
  6.5 169.1 %copy-start.1 = (bf16[256,256]{1,0:T(8,128)(2,1)S(1)}, bf16[256,256]{1,0:T(8,128)(2,1)}, u32[]{:S(2)}) copy-start(bf16[256,256]{1,0:T(8,128)(2,1)} %param.13) | copy-start | bytes 393220
  6.5 185.5 %copy-start = (f32[2048]{0:T(1024)S(1)}, f32[2048]{0:T(1024)}, u32[]{:S(2)}) copy-start(f32[2048]{0:T(1024)} %param.15) | copy-start | bytes 24580
  6.6 185.5 %all-gather.2.cloned.1.call-start = ((), (), s32[]{:S(2)}) async-start(), calls=%async_computation.4 | async-start | bytes 8650752 | tf_op jit(solution)/shard_map/all_gather | solution.py:322
  10.1 94.0 %all-to-all-start = ((bf16[4,256,256]{2,1,0:T(8,128)(2,1)}), bf16[4,256,256]{2,1,0:T(8,128)(2,1)S(1)}, u32[]{:S(2)}, u32[]{:S(2)}) async-start(bf16[4,256,256]{2,1,0:T(8,128)(2,1)} %broadcast_in_dim.18), calls=%async_computation | async-start | bytes 1048576 | tf_op jit(solution)/shard_map/all_to_all | solution.py:28
  96.7 24.5 %collective-permute-start.1 = (bf16[512,384]{1,0:T(8,128)(2,1)S(1)}, bf16[512,384]{1,0:T(8,128)(2,1)S(1)}, u32[]{:S(2)}, u32[]{:S(2)}) collective-permute-start(bf16[512,384]{1,0:T(8,128)(2,1)S(1)} %get-tuple-element.18.refs_1_), channel_id=1, source_target_pairs={{0,8},{8,16},{16,24},{24,32},{32,40},{40,48},{48,56},{56,64},{64,7... | collective-permute-start | bytes 1179656 | tf_op jit(solution)/shard_map/ppermute | solution.py:96
  100.8 23.8 %collective-permute-start.4 = (bf16[512,384]{1,0:T(8,128)(2,1)S(1)}, bf16[512,384]{1,0:T(8,128)(2,1)S(1)}, u32[]{:S(2)}, u32[]{:S(2)}) collective-permute-start(bf16[512,384]{1,0:T(8,128)(2,1)S(1)} %get-tuple-element.17.refs_5_), channel_id=1, source_target_pairs={{0,248},{8,0},{16,8},{24,16},{32,24},{40,32},{48,40},{56,48},{64,5... | collective-permute-start | bytes 1179656 | tf_op jit(solution)/shard_map/ppermute | solution.py:96
  104.2 50.0 %collective-permute-start.6 = (bf16[4,256,256]{2,1,0:T(8,128)(2,1)S(1)}, bf16[4,256,256]{2,1,0:T(8,128)(2,1)S(1)}, u32[]{:S(2)}, u32[]{:S(2)}) collective-permute-start(bf16[4,256,256]{2,1,0:T(8,128)(2,1)S(1)} %all-to-all-done.refs_9_), channel_id=1, source_target_pairs={{0,1},{1,0},{2,3},{3,2},{4,5},{5,4},{6,7},{7,6},{8,9},{9,8},{10,11... | collective-permute-start | bytes 1572872 | tf_op jit(solution)/shard_map/ppermute | solution.py:22
  113.9 15.0 %collective-permute-start = (bf16[512,384]{1,0:T(8,128)(2,1)S(1)}, bf16[512,384]{1,0:T(8,128)(2,1)S(1)}, u32[]{:S(2)}, u32[]{:S(2)}) collective-permute-start(bf16[512,384]{1,0:T(8,128)(2,1)S(1)} %get-tuple-element.18.refs_1_), channel_id=1, source_target_pairs={{0,256},{256,0},{1,257},{257,1},{2,258},{258,2},{3,259},{259,3},{4... | collective-permute-start | bytes 1179656 | tf_op jit(solution)/shard_map/ppermute | solution.py:76
  119.3 18.0 %collective-permute-start.3 = (bf16[512,384]{1,0:T(8,128)(2,1)S(1)}, bf16[512,384]{1,0:T(8,128)(2,1)S(1)}, u32[]{:S(2)}, u32[]{:S(2)}) collective-permute-start(bf16[512,384]{1,0:T(8,128)(2,1)S(1)} %get-tuple-element.17.refs_5_), channel_id=1, source_target_pairs={{0,256},{256,0},{1,257},{257,1},{2,258},{258,2},{3,259},{259,3},{4... | collective-permute-start | bytes 1179656 | tf_op jit(solution)/shard_map/ppermute | solution.py:76
  121.3 24.5 %collective-permute-start.2 = (bf16[512,384]{1,0:T(8,128)(2,1)S(1)}, bf16[512,384]{1,0:T(8,128)(2,1)}, u32[]{:S(2)}, u32[]{:S(2)}) collective-permute-start(bf16[512,384]{1,0:T(8,128)(2,1)S(1)} %collective-permute-done.1.refs_3_), channel_id=1, source_target_pairs={{0,256},{256,0},{1,257},{257,1},{2,258},{258,2},{3,259},{259,3},{4... | collective-permute-start | bytes 1179656 | tf_op jit(solution)/shard_map/ppermute | solution.py:76
  124.7 29.5 %collective-permute-start.5 = (bf16[512,384]{1,0:T(8,128)(2,1)S(1)}, bf16[512,384]{1,0:T(8,128)(2,1)}, u32[]{:S(2)}, u32[]{:S(2)}) collective-permute-start(bf16[512,384]{1,0:T(8,128)(2,1)S(1)} %collective-permute-done.4.refs_7_), channel_id=1, source_target_pairs={{0,256},{256,0},{1,257},{257,1},{2,258},{258,2},{3,259},{259,3},{4... | collective-permute-start | bytes 1179656 | tf_op jit(solution)/shard_map/ppermute | solution.py:76
  159.1 4.0 %collective-permute-start.7 = (bf16[4,256,256]{2,1,0:T(8,128)(2,1)S(1)}, bf16[4,256,256]{2,1,0:T(8,128)(2,1)S(1)}, u32[]{:S(2)}, u32[]{:S(2)}) collective-permute-start(bf16[4,256,256]{2,1,0:T(8,128)(2,1)S(1)} %get-tuple-element.13), channel_id=1, source_target_pairs={{0,1},{1,0},{2,3},{3,2},{4,5},{5,4},{6,7},{7,6},{8,9},{9,8},{10,11... | collective-permute-start | bytes 1572872 | tf_op jit(solution)/shard_map/ppermute | solution.py:22
  186.0 6.1 %collective-permute-start.8 = (bf16[4,256,256]{2,1,0:T(8,128)(2,1)S(1)}, bf16[4,256,256]{2,1,0:T(8,128)(2,1)S(1)}, u32[]{:S(2)}, u32[]{:S(2)}) collective-permute-start(bf16[4,256,256]{2,1,0:T(8,128)(2,1)S(1)} %all_to_all.21.mine), channel_id=1, source_target_pairs={{0,1},{1,0},{2,3},{3,2},{4,5},{5,4},{6,7},{7,6},{8,9},{9,8},{10,11... | collective-permute-start | bytes 1572872 | tf_op jit(solution)/shard_map/ppermute | solution.py:22
  197.5 7.8 %collective-permute-start.9 = (bf16[4,256,256]{2,1,0:T(8,128)(2,1)S(1)}, bf16[4,256,256]{2,1,0:T(8,128)(2,1)S(1)}, u32[]{:S(2)}, u32[]{:S(2)}) collective-permute-start(bf16[4,256,256]{2,1,0:T(8,128)(2,1)S(1)} %get-tuple-element.16), channel_id=1, source_target_pairs={{0,1},{1,0},{2,3},{3,2},{4,5},{5,4},{6,7},{7,6},{8,9},{9,8},{10,11... | collective-permute-start | bytes 1572872 | tf_op jit(solution)/shard_map/ppermute | solution.py:22
Sparse Core Ops, SparseCore 0:
  9.4 172.3 all-gather.1
